TPU v7x, 256 devices: a whole 4x4x8 slice. The times are simulated.
256 devices in a mesh: tp: 32 (over z, y), dp: 8 (over x, core).
Axes of the slice: x: 4, y: 4, z: 8, core: 2. Of those that a mesh axis runs over, the one named last changes fastest.
Arguments:
- tokens: bfloat16 [192, 1024], P('tp', 'dp'), may hold values from -6 to 6
- lengths: int32 [192], P('dp'), may hold values from 1 to 8, 384 in all
- norm_gain: float32 [2, 1024], P(None, 'dp'), may hold values from 0.1 to 1.9
- w_gate: bfloat16 [2, 1024, 2048], P(None, 'dp', 'tp'), may hold values from -0.1875 to 0.1875
- w_value: bfloat16 [2, 1024, 2048], P(None, 'dp', 'tp'), may hold values from -0.1875 to 0.1875
- w_write: bfloat16 [2, 1024, 256], P(None, 'dp', 'tp'), may hold values from -0.1875 to 0.1875
- w_read: bfloat16 [2, 1024, 256], P(None, 'dp', 'tp'), may hold values from -0.1875 to 0.1875
- w_step: bfloat16 [2, 1024, 32], P(None, 'dp', 'tp'), may hold values from -0.1875 to 0.1875
- step_bias: float32 [2, 32], P(None, 'tp'), may hold values from -1 to 1
- decay_rate: float32 [2, 32], P(None, 'tp'), may hold values from 0.5 to 4
- skip_gain: float32 [2, 32], P(None, 'tp'), may hold values from 0.5 to 2
- conv_value_w: float32 [2, 4, 2048], P(None, None, 'tp'), may hold values from -3 to 3
- conv_write_w: float32 [2, 4, 256], P(None, None, 'tp'), may hold values from -3 to 3
- conv_read_w: float32 [2, 4, 256], P(None, None, 'tp'), may hold values from -3 to 3
- group_gain: float32 [2, 2048], P(None, 'tp'), may hold values from 0.1 to 1.9
- w_out: bfloat16 [2, 2048, 1024], P(None, 'tp', 'dp'), may hold values from -0.125 to 0.125
- state: float32 [2, 192, 32, 64, 128], P(None, 'dp', 'tp'), may hold values from -0.6 to 0.6
- hist_value: bfloat16 [2, 192, 3, 2048], P(None, 'dp', None, 'tp'), may hold values from -6 to 6
- hist_write: bfloat16 [2, 192, 3, 256], P(None, 'dp', None, 'tp'), may hold values from -6 to 6
- hist_read: bfloat16 [2, 192, 3, 256], P(None, 'dp', None, 'tp'), may hold values from -6 to 6
Outputs:
- mixed: float32 [192, 1024], P('tp', 'dp')
- new_state: float32 [2, 192, 32, 64, 128], P(None, 'dp', 'tp')
- new_hist_value: bfloat16 [2, 192, 3, 2048], P(None, 'dp', None, 'tp')
- new_hist_write: bfloat16 [2, 192, 3, 256], P(None, 'dp', None, 'tp')
- new_hist_read: bfloat16 [2, 192, 3, 256], P(None, 'dp', None, 'tp')
Inputs may be any that keep to these rules, and one draw needn't show every extreme that they name: `lengths`: each sequence holds between 1 and 8 tokens before this step, and some sequence holds exactly 8.
All inputs are finite; a program needn't handle non-finite values.
Results may differ from a plain program's by a relative error of at most 0.03.
Values may be sent and summed in bfloat16 or wider, within the bound.
A program may use at most 64 MiB of HBM per device.

v0:
```python
import functools

import jax
import jax.numpy as jnp
from jax import lax
from jax.sharding import Mesh
from jax.sharding import PartitionSpec as P

D = 1024
GROUPS = 2
TP = ("tp_0", "tp_1")


norm_eps = 1e-05


def whole_of(x, axes, dim):
    if not axes:
        return x
    nearer = lax.all_gather(x, axes[-1], axis=dim, tiled=True)
    return whole_of(nearer, axes[:-1], dim)


def joined_along(pieces, dim):
    dims = list(pieces.shape[1:])
    dims[dim] *= pieces.shape[0]
    return jnp.moveaxis(pieces, 0, dim).reshape(dims)


def gather_together(arrays, axis, dims):
    vector = jnp.concatenate([a.reshape(-1) for a in arrays])
    lines, at, gathered = lax.all_gather(vector, axis), 0, []
    for a, dim in zip(arrays, dims):
        pieces = lines[:, at : at + a.size].reshape(-1, *a.shape)
        gathered.append(joined_along(pieces, dim))
        at += a.size
    return tuple(gathered)


def over_axes(x, axes):
    return functools.reduce(lax.psum, axes, x)


def scatter_axes(x, axes, dim):
    for axis in axes:
        x = lax.psum_scatter(x, axis, scatter_dimension=dim, tiled=True)
    return x


def conv_update(history, current, conv_taps, live_mask):
    kept_hist = history.astype(jnp.float32) * live_mask[:, :, None]
    mixed_sum = (
        jnp.sum(kept_hist * conv_taps[None, :-1, :], axis=1)
        + current.astype(jnp.float32) * conv_taps[-1][None, :]
    )
    fresh_hist = jnp.concatenate(
        [kept_hist[:, 1:].astype(jnp.bfloat16), current[:, None, :]], axis=1
    )
    return (jax.nn.silu(mixed_sum), fresh_hist)


def local(
    tokens,
    lengths,
    norm_gain,
    w_gate,
    w_value,
    w_write,
    w_read,
    w_step,
    step_bias,
    decay_rate,
    skip_gain,
    conv_value_w,
    conv_write_w,
    conv_read_w,
    group_gain,
    w_out,
    state,
    hist_value,
    hist_write,
    hist_read,
):
    seq_here = state.shape[1]
    local_heads = state.shape[2]
    head_dim = state.shape[3]
    hist_len = hist_value.shape[2]
    all_heads = local_heads * lax.axis_size(TP)
    per_group = all_heads // GROUPS
    group_width = all_heads * head_dim // GROUPS
    heads_here = lax.axis_index(TP) * local_heads + jnp.arange(local_heads, dtype=jnp.int32)
    group_here = heads_here // per_group
    member = (group_here[:, None] == jnp.arange(GROUPS, dtype=jnp.int32)[None, :]).astype(
        jnp.float32
    )
    offsets = hist_len - jnp.arange(hist_len, dtype=jnp.int32)
    live_mask = (offsets[None, :] <= lengths[:, None]).astype(jnp.float32)
    gate_cols = w_gate.shape[2]
    value_cols = w_value.shape[2]
    write_cols = w_write.shape[2]
    read_cols = w_read.shape[2]
    gathered = whole_of(tokens, TP, 0).astype(jnp.float32)
    current = tokens
    states_out, values_out, writes_out, reads_out = ([], [], [], [])
    for layer_idx in range(2):
        row_squares = jnp.sum(gathered * gathered, axis=1)
        weights = jnp.concatenate(
            [
                w_gate[layer_idx],
                w_value[layer_idx],
                w_write[layer_idx],
                w_read[layer_idx],
                w_step[layer_idx],
            ],
            axis=1,
        )
        total_sq = lax.psum(row_squares, "dp")
        row_scale = lax.rsqrt(total_sq / D + norm_eps)
        normed = (gathered * row_scale[:, None] * norm_gain[layer_idx][None, :]).astype(
            jnp.bfloat16
        )

        def project():
            row_block = lax.slice_in_dim(normed, 0, seq_here * lax.axis_size("dp"), axis=0)
            return jnp.dot(row_block, weights, preferred_element_type=jnp.float32)

        mixed_in = lax.psum_scatter(project(), "dp", scatter_dimension=0, tiled=True)
        edge_one = gate_cols
        edge_two = edge_one + value_cols
        edge_three = edge_two + write_cols
        edge_four = edge_three + read_cols
        gate_part = mixed_in[:, :edge_one].astype(jnp.bfloat16)
        value_part = mixed_in[:, edge_one:edge_two].astype(jnp.bfloat16)
        write_part = mixed_in[:, edge_two:edge_three].astype(jnp.bfloat16)
        read_part = mixed_in[:, edge_three:edge_four].astype(jnp.bfloat16)
        step_raw = mixed_in[:, edge_four:]
        value_act, value_hist = conv_update(
            hist_value[layer_idx], value_part, conv_value_w[layer_idx], live_mask
        )
        write_act, write_hist = conv_update(
            hist_write[layer_idx], write_part, conv_write_w[layer_idx], live_mask
        )
        read_act, read_hist = conv_update(
            hist_read[layer_idx], read_part, conv_read_w[layer_idx], live_mask
        )
        write_all, read_all = gather_together((write_act, read_act), TP, (1, 1))
        write_heads = jnp.moveaxis(
            jnp.take(write_all.reshape(seq_here, -1, GROUPS), group_here, axis=2), 2, 1
        )
        read_heads = jnp.moveaxis(
            jnp.take(read_all.reshape(seq_here, -1, GROUPS), group_here, axis=2), 2, 1
        )
        step_size = jax.nn.softplus(step_raw + step_bias[layer_idx][None, :])
        decay_keep = jnp.exp(-decay_rate[layer_idx][None, :] * step_size)
        inputs = value_act.reshape(seq_here, local_heads, head_dim)
        updated = (
            decay_keep[:, :, None, None] * state[layer_idx]
            + (step_size[:, :, None] * inputs)[:, :, :, None] * write_heads[:, :, None, :]
        )
        readout = (
            jnp.einsum("shpn,shn->shp", updated, read_heads, precision=lax.Precision.DEFAULT)
            + skip_gain[layer_idx][None, :, None] * inputs
        )
        gated_out = readout * jax.nn.silu(gate_part.astype(jnp.float32)).reshape(
            seq_here, local_heads, head_dim
        )
        head_squares = jnp.sum(gated_out * gated_out, axis=2)
        group_squares = jnp.dot(head_squares, member, precision=lax.Precision.DEFAULT)
        group_total = over_axes(group_squares, TP)
        group_scale = lax.rsqrt(group_total / group_width + norm_eps)
        head_scale = jnp.take(group_scale, group_here, axis=1)
        scaled_out = (gated_out * head_scale[:, :, None]).reshape(seq_here, -1)
        mixer_out = (scaled_out * group_gain[layer_idx][None, :]).astype(jnp.bfloat16)
        proj_out = w_out[layer_idx]

        def emit_rows(shard_rows):
            return jnp.dot(shard_rows, proj_out, preferred_element_type=jnp.float32)

        partial_value = emit_rows(lax.all_gather(mixer_out, "dp", axis=0, tiled=True))
        if layer_idx == 0:
            rounded = lax.optimization_barrier(over_axes(partial_value, TP).astype(jnp.bfloat16))
            gathered = rounded.astype(jnp.float32)
        else:
            current = scatter_axes(partial_value, TP, 0)
        states_out.append(updated)
        values_out.append(value_hist)
        writes_out.append(write_hist)
        reads_out.append(read_hist)
    return (
        current,
        jnp.stack(states_out),
        jnp.stack(values_out),
        jnp.stack(writes_out),
        jnp.stack(reads_out),
    )


def solution(mesh):
    torus = Mesh(mesh.devices.reshape(8, 4, mesh.shape["dp"]), ("tp_0", "tp_1", "dp"))
    return jax.shard_map(
        local,
        mesh=torus,
        in_specs=(
            P(TP, "dp"),
            P("dp"),
            P(None, "dp"),
            P(None, "dp", TP),
            P(None, "dp", TP),
            P(None, "dp", TP),
            P(None, "dp", TP),
            P(None, "dp", TP),
            P(None, TP),
            P(None, TP),
            P(None, TP),
            P(None, None, TP),
            P(None, None, TP),
            P(None, None, TP),
            P(None, TP),
            P(None, TP, "dp"),
            P(None, "dp", TP, None, None),
            P(None, "dp", None, TP),
            P(None, "dp", None, TP),
            P(None, "dp", None, TP),
        ),
        out_specs=(
            P(TP, "dp"),
            P(None, "dp", TP, None, None),
            P(None, "dp", None, TP),
            P(None, "dp", None, TP),
            P(None, "dp", None, TP),
        ),
        check_vma=False,
    )
```

profile of v0, /device:TPU:2, one launch (start us, length us, event | category | flops | bytes accessed | tf_op | source)
XLA Modules:
  0.0 469.3 jit_solution(14598672917770624518)
XLA Ops:
  7.2 0.8 slice_bitcast_fusion.20
  8.0 12.5 %all-gather.2 = bf16[4,6,128]{2,1,0:T(8,128)(2,1)S(1)} all-gather(bf16[1,6,128]{2,1,0:T(8,128)(2,1)} %bitcast.209), channel_id=1, replica_groups=mesh['tp_0'=8,'tp_1'=4,'dp'=8] {'tp_1'}, dimensions={0}, use_global_device_ids=true | all-gather | bytes 7680 | tf_op jit(solution)/shard_map/all_gather | solution.py:20
  20.4 28.1 %all_gather.25 = bf16[192,128]{1,0:T(8,128)(2,1)S(1)} all-gather(bf16[24,128]{1,0:T(8,128)(2,1)S(1)} %reshape.410), channel_id=1, replica_groups=mesh['tp_0'=8,'tp_1'=4,'dp'=8] {'tp_0'}, dimensions={0}, use_global_device_ids=true | all-gather | bytes 55296 | tf_op jit(solution)/shard_map/all_gather | solution.py:20
  48.6 0.1 fusion.16
  48.7 10.1 %psum.56 = f32[192]{0:T(256)S(1)} all-reduce(f32[192]{0:T(256)S(1)} %fusion.16), channel_id=1, replica_groups=mesh['tp_0'=8,'tp_1'=4,'dp'=8] {'dp'}, use_global_device_ids=true, to_apply=%region_1.2 | all-reduce | flops 192 | bytes 1536 | tf_op jit(solution)/shard_map/psum | solution.py:117
  58.8 0.7 constant_dynamic-update-slice_fusion.4
  59.6 0.7 constant_dynamic-update-slice_fusion.3
  60.3 0.7 constant_dynamic-update-slice_fusion.2
  61.0 0.7 constant_dynamic-update-slice_fusion.1
  61.7 0.7 constant_dynamic-update-slice_fusion
  62.5 0.9 fusion.24
  63.5 0.7 slice_bitcast_fusion.19
  64.2 0.7 slice_bitcast_fusion.11
  64.9 0.7 slice_bitcast_fusion.17
  65.6 0.7 slice_bitcast_fusion.9
  66.4 1.3 fusion.48
  67.7 1.3 fusion.49
  70.3 1.3 fusion.50
  71.6 0.7 compare_convert_fusion.1
  72.3 0.8 convert_multiply_fusion.7
  73.1 0.8 multiply_reduce_fusion
  74.1 0.8 convert_multiply_fusion.10
  75.0 1.3 dynamic-slice.20
  76.9 0.8 multiply_reduce_fusion.5
  77.7 0.8 slice_bitcast_fusion.16
  78.5 14.3 %reduce-scatter.10.cloned.1.call-done = f32[24,145]{1,0:T(8,128)} async-done(((f32[192,145]{1,0:T(8,128)}), f32[24,145]{1,0:T(8,128)}) %reduce-scatter.10.cloned.1.call-update) | async-done | bytes 13936
  92.7 0.8 copy.142
  94.1 49.9 %all-gather.3 = f32[32,1,384]{2,1,0:T(1,128)S(1)} all-gather(f32[1,1,384]{2,1,0:T(1,128)S(1)} %reshape.411), channel_id=2, replica_groups=mesh['tp_0'=8,'tp_1'=4,'dp'=8] {'tp_0','tp_1'}, dimensions={0}, use_global_device_ids=true | all-gather | bytes 50688 | tf_op jit(solution)/shard_map/all_gather | solution.py:32
  144.0 0.1 copy.110
  144.2 0.6 exponential_bitcast_fusion.1
  145.0 0.1 copy.113
  145.3 0.1 copy.111
  145.6 0.4 fusion.4
  146.1 0.8 multiply_reduce_fusion.3
  147.0 16.0 %psum.57 = f32[24,2]{0,1:T(2,128)S(1)} all-reduce(f32[24,2]{0,1:T(2,128)S(1)} %broadcast_multiply_fusion.3), channel_id=1, replica_groups=mesh['tp_0'=8,'tp_1'=4,'dp'=8] {'tp_0'}, use_global_device_ids=true, to_apply=%region_7.9 | all-reduce | flops 48 | bytes 384 | tf_op jit(solution)/shard_map/psum | solution.py:41
  163.0 9.1 %psum.58 = f32[24,2]{0,1:T(2,128)S(1)} all-reduce(f32[24,2]{0,1:T(2,128)S(1)} %psum.57), channel_id=1, replica_groups=mesh['tp_0'=8,'tp_1'=4,'dp'=8] {'tp_1'}, use_global_device_ids=true, to_apply=%region_8.10 | all-reduce | flops 48 | bytes 384 | tf_op jit(solution)/shard_map/psum | solution.py:41
  172.2 13.0 %all_gather.28 = bf16[192,64]{1,0:T(8,128)(2,1)S(1)} all-gather(bf16[24,64]{1,0:T(8,128)(2,1)S(1)} %copy.115), channel_id=1, replica_groups=mesh['tp_0'=8,'tp_1'=4,'dp'=8] {'dp'}, dimensions={0}, use_global_device_ids=true | all-gather | bytes 27648 | tf_op jit(solution)/shard_map/all_gather | solution.py:179
  185.2 0.8 fusion.40
  186.2 71.3 %all-reduce.4.cloned.1.call-done = f32[192,128]{1,0:T(8,128)} async-done(((f32[192,128]{1,0:T(8,128)}), f32[192,128]{1,0:T(8,128)}) %all-reduce.4.cloned.1.call-update) | async-done | bytes 98320 | tf_op jit(solution)/shard_map/psum | solution.py:41
  257.5 18.4 %psum.60 = bf16[192,128]{1,0:T(8,128)(2,1)S(1)} all-reduce(f32[192,128]{1,0:T(8,128)} %all-reduce.4.cloned.1.call-done), channel_id=1, replica_groups=mesh['tp_0'=8,'tp_1'=4,'dp'=8] {'tp_1'}, use_global_device_ids=true, to_apply=%region_10.13 | all-reduce | flops 24576 | bytes 147456 | tf_op jit(solution)/shard_map/psum | solution.py:41
  275.9 0.1 fusion.19
  276.0 10.0 %psum.61 = f32[192]{0:T(256)S(1)} all-reduce(f32[192]{0:T(256)S(1)} %fusion.19), channel_id=1, replica_groups=mesh['tp_0'=8,'tp_1'=4,'dp'=8] {'dp'}, use_global_device_ids=true, to_apply=%region_12.15 | all-reduce | flops 192 | bytes 1536 | tf_op jit(solution)/shard_map/psum | solution.py:117
  286.0 0.9 fusion.22
  287.0 27.8 %reduce-scatter.12.cloned.1.call-done = f32[24,145]{1,0:T(8,128)} async-done(((f32[192,145]{1,0:T(8,128)}), f32[24,145]{1,0:T(8,128)}) %reduce-scatter.12.cloned.1.call-update) | async-done | bytes 13936
  314.8 0.8 copy.144
  316.2 50.0 %all-gather.4 = f32[32,1,384]{2,1,0:T(1,128)S(1)} all-gather(f32[1,1,384]{2,1,0:T(1,128)S(1)} %reshape.413), channel_id=3, replica_groups=mesh['tp_0'=8,'tp_1'=4,'dp'=8] {'tp_0','tp_1'}, dimensions={0}, use_global_device_ids=true | all-gather | bytes 50688 | tf_op jit(solution)/shard_map/all_gather | solution.py:32
  366.2 0.1 copy.121
  366.4 0.6 exponential_bitcast_fusion
  367.2 0.1 copy.124
  367.5 0.1 copy.122
  367.8 0.6 multiply_add_fusion.1
  368.4 0.4 fusion.1
  368.9 0.8 multiply_reduce_fusion.2
  369.7 15.9 %psum.62 = f32[24,2]{0,1:T(2,128)S(1)} all-reduce(f32[24,2]{0,1:T(2,128)S(1)} %broadcast_multiply_fusion.2), channel_id=1, replica_groups=mesh['tp_0'=8,'tp_1'=4,'dp'=8] {'tp_0'}, use_global_device_ids=true, to_apply=%region_18.21 | all-reduce | flops 48 | bytes 384 | tf_op jit(solution)/shard_map/psum | solution.py:41
  385.7 9.1 %psum.63 = f32[24,2]{0,1:T(2,128)S(1)} all-reduce(f32[24,2]{0,1:T(2,128)S(1)} %psum.62), channel_id=1, replica_groups=mesh['tp_0'=8,'tp_1'=4,'dp'=8] {'tp_1'}, use_global_device_ids=true, to_apply=%region_19.22 | all-reduce | flops 48 | bytes 384 | tf_op jit(solution)/shard_map/psum | solution.py:41
  395.0 13.1 %all_gather.31 = bf16[192,64]{1,0:T(8,128)(2,1)S(1)} all-gather(bf16[24,64]{1,0:T(8,128)(2,1)S(1)} %copy.126), channel_id=1, replica_groups=mesh['tp_0'=8,'tp_1'=4,'dp'=8] {'dp'}, dimensions={0}, use_global_device_ids=true | all-gather | bytes 27648 | tf_op jit(solution)/shard_map/all_gather | solution.py:179
  408.0 0.8 fusion.38
  408.8 0.6 pad_maximum_fusion.3
  409.4 0.6 pad_maximum_fusion.1
  410.1 0.6 pad_maximum_fusion.2
  410.7 1.2 pad_maximum_fusion
  411.9 32.8 %reduce-scatter.14.cloned.1.call-done = f32[24,128]{1,0:T(8,128)} async-done(((f32[192,128]{1,0:T(8,128)}), f32[24,128]{1,0:T(8,128)}) %reduce-scatter.14.cloned.1.call-update) | async-done | bytes 12304
  444.7 17.5 %all-reduce.1 = f32[24,128]{1,0:T(8,128)S(1)} all-reduce(f32[24,128]{1,0:T(8,128)} %reduce-scatter.14.cloned.1.call-done), channel_id=7, replica_groups=mesh['tp_0'=8,'tp_1'=4,'dp'=8] {'tp_1'}, use_global_device_ids=true, to_apply=%region_21.24.clone | all-reduce | flops 3072 | bytes 24576
  462.2 0.6 constant_dynamic-slice_fusion.2
  (80 shorter events, 3.3 us)
Async XLA Ops:
  7.2 85.6 %reduce-scatter.10.cloned.1.call-start = ((), (), s32[]{:S(2)}) async-start(), calls=%async_computation.4 | async-start | bytes 221184
  48.6 97.0 %copy-start = (f32[2,24,1,64,128]{4,3,2,1,0:T(8,128)S(1)}, f32[2,24,1,64,128]{4,3,2,1,0:T(8,128)}, u32[]{:S(2)}) copy-start(f32[2,24,1,64,128]{4,3,2,1,0:T(8,128)} %param.40) | copy-start | bytes 4718596
  63.4 194.1 %all-reduce.4.cloned.1.call-start = ((), (), s32[]{:S(2)}) async-start(), calls=%async_computation.3 | async-start | bytes 196608 | tf_op jit(solution)/shard_map/psum | solution.py:41
  78.5 106.8 %copy-start.1 = (bf16[2,64,128]{2,1,0:T(8,128)(2,1)S(1)}, bf16[2,64,128]{2,1,0:T(8,128)(2,1)}, u32[]{:S(2)}) copy-start(bf16[2,64,128]{2,1,0:T(8,128)(2,1)} %param.39) | copy-start | bytes 98308
  186.0 128.8 %reduce-scatter.12.cloned.1.call-start = ((), (), s32[]{:S(2)}) async-start(), calls=%async_computation.5 | async-start | bytes 221184
  287.0 157.7 %reduce-scatter.14.cloned.1.call-start = ((), (), s32[]{:S(2)}) async-start(), calls=%async_computation.6 | async-start | bytes 110592
Sparse Core Ops, SparseCore 0:
  63.5 29.1 reduce-scatter.9
  186.2 71.2 all-reduce.3
  287.1 27.6 reduce-scatter.11
  408.9 35.7 reduce-scatter.13
where the time goes:
time: 471 us; the launch traced here: 469 us
  blocking collectives  273 us (58%)
  waiting for transfers between devices  146 us (31%)
  local copies, waits for them, and re-layouts  18.1 us (4%)
  between operations  16.1 us (3%)
  other arithmetic  11.9 us (3%)
    all_gather x2, blocking collectives, gather_together(): lines, at, gathered = (lax.all_gather(vector, axis), 0, [])  99.9 us
    unnamed x7, waiting for transfers between devices  74.9 us
    psum x1, waiting for transfers between devices, over_axes(): return functools.reduce(lax.psum, axes, x)  71.3 us
    psum x5, blocking collectives, over_axes(): return functools.reduce(lax.psum, axes, x)  68.5 us
    all_gather x2, blocking collectives, whole_of(): nearer = lax.all_gather(x, axes[-1], axis=dim, tiled=True)  40.6 us
    all_gather x2, blocking collectives, local(): lax.all_gather(mixer_out, 'dp', axis=0, tiled=True)  26.1 us
    psum x2, blocking collectives, local(): total_sq = lax.psum(row_squares, 'dp')  20.1 us
    unnamed x1, blocking collectives  17.5 us
  transfers between devices with their start and end apart: 4, of which 4 were waited for; matrix products, arithmetic and copies ran while one was open for 3% of the time, Pallas kernels for 0%

commit v1 on v0

v1 whole, which is shorter than its diff:
```python
import jax
import jax.numpy as jnp
from jax import lax
from jax.experimental import pallas as pl
from jax.experimental.pallas import tpu as pltpu
from jax.sharding import PartitionSpec as P

MESH = pl.DeviceIdType.MESH
F32 = jnp.float32
BF16 = jnp.bfloat16

NTP = 32
NDP = 8
PER = 6
PAD = 8
NBLK = 4
ROWS = NBLK * PAD
SEQ = NBLK * PER
HD = 64
ST = 128
D = 1024
GW = 1024.0
EPS = 1e-05
NW = 160

NT = (((1,), (1,)), ((), ()))
TN = (((0,), (0,)), ((), ()))
NN = (((1,), (0,)), ((), ()))


def dot(a, b, dims):
    return lax.dot_general(a, b, dims, preferred_element_type=F32)


def iota(shape, dim):
    return lax.broadcasted_iota(jnp.int32, shape, dim)


def silu(x):
    return x / (1.0 + jnp.exp(-x))


def column(row, rows):
    wide = jnp.broadcast_to(row, (rows, row.shape[1]))
    pick = iota(wide.shape, 1) == iota(wide.shape, 0)
    return jnp.sum(jnp.where(pick, wide, 0.0), axis=1, keepdims=True)


def kernel(
    tok_ref,
    len_ref,
    gain_ref,
    wg_ref,
    wv_ref,
    ww_ref,
    wr_ref,
    ws_ref,
    bias_ref,
    rate_ref,
    skip_ref,
    cv_ref,
    cw_ref,
    cr_ref,
    gg_ref,
    wo_ref,
    st_hbm,
    hv_ref,
    hw_ref,
    hr_ref,
    mixed_ref,
    nst_hbm,
    nhv_ref,
    nhw_ref,
    nhr_ref,
    st,
    xbuf,
    wbuf,
    wobuf,
    tok_send,
    map_send,
    map_buf,
    part_send,
    part_buf,
    pre_v,
    pre_m,
    sel,
    wr_all,
    st_sem,
    out_sem,
    tok_s,
    tok_r,
    win_s,
    win_r,
    wo_s,
    wo_r,
    map_s,
    map_r,
    part_s,
    part_r,
    ag_s,
    ag_r,
):
    t = lax.axis_index("tp")
    d = lax.axis_index("dp")
    mine = (t // NBLK) == d

    def when_mine(i_tp, i_dp, fn_other):
        pl.when(jnp.logical_or(i_tp != t, i_dp != d))(fn_other)

    barrier = pltpu.get_barrier_semaphore()

    def tell(i_tp, i_dp):
        pl.semaphore_signal(barrier, inc=1, device_id=(i_tp, i_dp), device_id_type=MESH)

    def greet(k, _):
        when_mine(k, t // NBLK, lambda: tell(k, t // NBLK))
        b_tp, b_dp = d * NBLK + k // NDP, k % NDP
        when_mine(b_tp, b_dp, lambda: tell(b_tp, b_dp))
        when_mine(k, d, lambda: tell(k, d))
        return 0

    lax.fori_loop(0, NTP, greet, 0)

    def greet_dp(k, _):
        tell(t, lax.rem(d + k, NDP))
        return 0

    lax.fori_loop(1, NDP, greet_dp, 0)

    st_copies = []
    for l in range(2):
        copy = pltpu.make_async_copy(st_hbm.at[l], st.at[l], st_sem.at[l])
        copy.start()
        st_copies.append(copy)

    tok_send[...] = jnp.concatenate(
        [tok_ref[...].astype(F32), jnp.zeros((PAD - PER, 128), F32)], axis=0
    ).astype(BF16)

    q_r, q_c = iota((16, 16), 0), iota((16, 16), 1)
    perm = jnp.where(
        q_c == ((q_r % 8) // 4) * 8 + 2 * (q_r % 4) + q_r // 8, 1.0, 0.0
    ).astype(BF16)
    p_r, p_c = iota((SEQ, ROWS), 0), iota((SEQ, ROWS), 1)
    spread = jnp.where(p_c == (p_r // PER) * PAD + p_r % PER, 1.0, 0.0).astype(BF16)

    r8 = iota((8, 128), 0)
    for l in range(2):
        maps = jnp.concatenate([ww_ref[l].astype(F32), wr_ref[l].astype(F32)], axis=0).astype(BF16)
        maps = dot(perm, maps, NN)
        gain = gain_ref[l : l + 1, :]
        high = gain.astype(BF16).astype(F32)
        low = gain - high
        step_row = ws_ref[l : l + 1, :].astype(F32)
        extra = jnp.where(
            r8 == 0, step_row, jnp.where(r8 == 1, high, jnp.where(r8 == 2, low, 0.0))
        )
        packed = jnp.concatenate([maps, extra, jnp.zeros((8, 128), F32)], axis=0)
        wbuf[l, d, pl.ds(128, 32), :] = packed.astype(BF16)
        wbuf[l, d, pl.ds(0, 64), :] = wg_ref[l]
        wbuf[l, d, pl.ds(64, 64), :] = wv_ref[l]
        wobuf[l, d] = wo_ref[l]

    s_r, s_c = iota((256, 256), 0), iota((256, 256), 1)
    sel[...] = jnp.where(
        s_c == ((s_r % 8) // 4) * 128 + (s_r // 8) * 4 + s_r % 4, 1.0, 0.0
    ).astype(BF16)

    len_row = len_ref[...].astype(F32)
    len_pad = dot(jnp.broadcast_to(len_row, (8, SEQ)).astype(BF16), spread, NN)[0:1, :]
    len_col = column(len_row, SEQ)
    live_row = [jnp.where(len_row >= 3.0 - k, 1.0, 0.0) for k in range(3)]
    live_pad = [jnp.where(len_pad >= 3.0 - k, 1.0, 0.0) for k in range(3)]
    live_col = [jnp.where(len_col >= 3.0 - k, 1.0, 0.0) for k in range(3)]

    c_r, c_c = iota((16, 8), 0), iota((16, 8), 1)
    c_pick = c_c == 2 * (c_r % 4) + c_r // 8
    c_kind = (c_r % 8) // 4
    tap_v, tap_m, gain_col = [], [], []
    for l in range(2):
        acc_v = jnp.zeros((HD, ROWS), F32)
        acc_m = jnp.zeros((16, ROWS), F32)
        for k in range(4):
            tv = column(cv_ref[l, k : k + 1, :], HD)
            both = jnp.where(c_kind == 0, cw_ref[l, k : k + 1, :], cr_ref[l, k : k + 1, :])
            tm = jnp.sum(jnp.where(c_pick, both, 0.0), axis=1, keepdims=True)
            if k == 3:
                tap_v.append(tv)
                tap_m.append(tm)
                continue
            acc_v = acc_v + dot(hv_ref[l, k], spread, TN) * live_pad[k] * tv
            hm = jnp.concatenate(
                [hw_ref[l, k].astype(F32), hr_ref[l, k].astype(F32)], axis=0
            ).astype(BF16)
            hm = dot(perm, hm, NN).astype(BF16)
            acc_m = acc_m + dot(hm, spread, NN) * live_pad[k] * tm
            if k > 0:
                nhv_ref[l, k - 1] = (hv_ref[l, k].astype(F32) * live_col[k]).astype(BF16)
                nhw_ref[l, k - 1] = (hw_ref[l, k].astype(F32) * live_row[k]).astype(BF16)
                nhr_ref[l, k - 1] = (hr_ref[l, k].astype(F32) * live_row[k]).astype(BF16)
        pre_v[l] = acc_v
        pre_m[l] = acc_m
        gain_col.append(column(gg_ref[l : l + 1, :], HD))

    pl.semaphore_wait(barrier, jnp.where(mine, 31 + 7 + 62, 31 + 7 + 64))

    own_slot = (t % NBLK) * NDP + d

    def push_tokens(k, _):
        dest = lax.rem(t + k, NTP)

        def go():
            pltpu.make_async_remote_copy(
                src_ref=tok_send,
                dst_ref=xbuf.at[0, own_slot],
                send_sem=tok_s,
                recv_sem=tok_r,
                device_id=(dest, t // NBLK),
                device_id_type=MESH,
            ).start()

        when_mine(dest, t // NBLK, go)
        return 0

    lax.fori_loop(0, NTP, push_tokens, 0)

    @pl.when(mine)
    def _():
        xbuf[0, own_slot] = tok_send[...]

    def push_in(l):
        def body(k, _):
            pltpu.make_async_remote_copy(
                src_ref=wbuf.at[l, d],
                dst_ref=wbuf.at[l, d],
                send_sem=win_s.at[l],
                recv_sem=win_r.at[l],
                device_id=(t, lax.rem(d + k, NDP)),
                device_id_type=MESH,
            ).start()
            return 0

        lax.fori_loop(1, NDP, body, 0)

    def push_wo(l):
        def body(k, _):
            pltpu.make_async_remote_copy(
                src_ref=wobuf.at[l, d],
                dst_ref=wobuf.at[l, d],
                send_sem=wo_s.at[l],
                recv_sem=wo_r.at[l],
                device_id=(t, lax.rem(d + k, NDP)),
                device_id_type=MESH,
            ).start()
            return 0

        lax.fori_loop(1, NDP, body, 0)

    push_in(0)
    push_wo(0)

    def wait_bytes(ref, sem):
        pltpu.make_async_copy(ref, ref, sem).wait()

    def wait_paired(ref_of, sem):
        @pl.when(mine)
        def _():
            wait_bytes(ref_of(NTP - 1), sem)

        @pl.when(jnp.logical_not(mine))
        def _():
            wait_bytes(ref_of(NTP), sem)

    row_of = iota((ROWS, 128), 0) % PAD
    lane32 = iota((HD, ROWS), 1)
    g = t // 16

    for l in range(2):
        if l == 0:
            wait_paired(lambda n: xbuf.at[0, pl.ds(0, n)], tok_r)
        else:
            wait_bytes(xbuf.at[1, pl.ds(0, NTP - 1)], ag_r)
        xs = []
        squares = jnp.zeros((ROWS, 128), F32)
        for c in range(NDP):
            x = jnp.concatenate(
                [xbuf[l, a * NDP + c].astype(F32) for a in range(NBLK)], axis=0
            )
            xs.append(x)
            squares = squares + x * x
        scale = lax.rsqrt(jnp.sum(squares, axis=1, keepdims=True) / D + EPS)
        wait_bytes(wbuf.at[l, pl.ds(0, NDP - 1)], win_r.at[l])
        proj = jnp.zeros((NW, ROWS), F32)
        for c in range(NDP):
            gains = wbuf[l, c, pl.ds(144, 16), :].astype(F32)
            gain = gains[1:2, :] + gains[2:3, :]
            normed = (xs[c] * scale * gain).astype(BF16)
            proj = proj + dot(wbuf[l, c], normed, NT)
        maps_new = proj[128:144, :].astype(BF16)
        maps_act = silu(pre_m[l] + maps_new.astype(F32) * tap_m[l])
        map_send[l, :, :, pl.ds(0, ROWS)] = maps_act.reshape(2, 8, ROWS).astype(BF16)

        def push_maps(k, _, l=l):
            dest = lax.rem(t + k, NTP)
            pltpu.make_async_remote_copy(
                src_ref=map_send.at[l, dest // 16],
                dst_ref=map_buf.at[l, t],
                send_sem=map_s.at[l],
                recv_sem=map_r.at[l],
                device_id=(dest, d),
                device_id_type=MESH,
            ).start()
            return 0

        lax.fori_loop(1, NTP, push_maps, 0)
        map_buf[l, t] = map_send[l, g]
        if l == 0:
            push_in(1)
            push_wo(1)

        gate = proj[0:64, :].astype(BF16).astype(F32)
        value_new = proj[64:128, :].astype(BF16)
        u = silu(pre_v[l] + value_new.astype(F32) * tap_v[l])
        raw = proj[144:145, :] + bias_ref[0:1, l : l + 1]
        step = jnp.maximum(raw, 0.0) + jnp.log1p(jnp.exp(-jnp.abs(raw)))
        keep = jnp.exp(-rate_ref[0:1, l : l + 1] * step)
        su = step * u
        sgate = silu(gate)

        nhv_ref[l, 2] = dot(spread, value_new, NT).astype(BF16)
        back = dot(perm, maps_new, TN).astype(BF16)
        back = dot(back, spread, NT)
        nhw_ref[l, 2] = back[0:8].astype(BF16)
        nhr_ref[l, 2] = back[8:16].astype(BF16)

        st_copies[l].wait()
        wait_bytes(map_buf.at[l, pl.ds(0, NTP - 1)], map_r.at[l])
        gathered = map_buf[l].astype(F32).reshape(NTP * 8, 128).astype(BF16)
        wr_all[...] = dot(gathered, sel[...], TN)[0:ROWS, :]

        read_out = jnp.zeros((HD, ROWS), F32)
        for s in range(SEQ):
            lane = (s // PER) * PAD + s % PER
            w_row = wr_all[lane : lane + 1, 0:ST]
            r_row = wr_all[lane : lane + 1, ST : 2 * ST]
            new = (
                keep[0:1, lane : lane + 1] * st[l, s] + su[:, lane : lane + 1] * w_row
            )
            st[l, s] = new
            got = jnp.sum(new * r_row, axis=1, keepdims=True)
            read_out = jnp.where(lane32 == lane, got, read_out)
        out_copy = pltpu.make_async_copy(st.at[l], nst_hbm.at[l], out_sem.at[l])
        out_copy.start()

        gated = (read_out + skip_ref[0:1, l : l + 1] * u) * sgate
        sq = jnp.sum(gated * gated, axis=0, keepdims=True)
        sq = jnp.concatenate([sq, jnp.zeros((1, 128 - ROWS), F32)], axis=1)
        sq_high = sq.astype(BF16).astype(F32)
        sq_low = sq - sq_high
        mix = (gated * gain_col[l]).astype(BF16)
        wait_bytes(wobuf.at[l, pl.ds(0, NDP - 1)], wo_r.at[l])
        for c in range(NDP):
            part = dot(mix, wobuf[l, c], TN)
            part = jnp.where(row_of == PER, sq_high, jnp.where(row_of == PER + 1, sq_low, part))
            part_send[l, c] = part.reshape(NBLK, PAD, 128).astype(BF16)

        if l == 0:

            def push_part(k, _):
                dest = lax.rem(t + k, NTP)
                pltpu.make_async_remote_copy(
                    src_ref=part_send.at[0, dest % NDP, dest // NDP],
                    dst_ref=part_buf.at[0, t],
                    send_sem=part_s.at[0],
                    recv_sem=part_r.at[0],
                    device_id=(dest, d),
                    device_id_type=MESH,
                ).start()
                return 0

            lax.fori_loop(1, NTP, push_part, 0)
            part_buf[0, t] = part_send[0, t % NDP, t // NDP]
            wait_bytes(part_buf.at[0, pl.ds(0, NTP - 1)], part_r.at[0])
            block = t // NDP
        else:

            def push_last(k, _):
                b = lax.rem(own_slot + k, NTP)
                dest_tp, dest_dp = d * NBLK + b // NDP, b % NDP

                def go():
                    pltpu.make_async_remote_copy(
                        src_ref=part_send.at[1, dest_dp, b // NDP],
                        dst_ref=part_buf.at[1, t],
                        send_sem=part_s.at[1],
                        recv_sem=part_r.at[1],
                        device_id=(dest_tp, dest_dp),
                        device_id_type=MESH,
                    ).start()

                when_mine(dest_tp, dest_dp, go)
                return 0

            lax.fori_loop(0, NTP, push_last, 0)

            @pl.when(mine)
            def _():
                part_buf[1, t] = part_send[1, d, t % NBLK]

            wait_paired(lambda n: part_buf.at[1, pl.ds(0, n)], part_r.at[1])
            block = t % NBLK

        total = jnp.zeros((PAD, 128), F32)
        for grp in range(2):
            acc = part_buf[l, grp * 16].astype(F32)
            for i in range(1, 16):
                acc = acc + part_buf[l, grp * 16 + i].astype(F32)
            both = acc[PER : PER + 1, :] + acc[PER + 1 : PER + 2, :]
            wide = jnp.broadcast_to(both, (PAD, 128))
            pick = iota((PAD, 128), 1) == block * PAD + iota((PAD, 128), 0)
            mean = jnp.sum(jnp.where(pick, wide, 0.0), axis=1, keepdims=True) / GW
            total = total + acc * lax.rsqrt(mean + EPS)

        if l == 0:
            total = jnp.where(iota((PAD, 128), 0) < PER, total, 0.0)
            xbuf[1, t] = total.astype(BF16)

            def push_out(k, _):
                pltpu.make_async_remote_copy(
                    src_ref=xbuf.at[1, t],
                    dst_ref=xbuf.at[1, t],
                    send_sem=ag_s,
                    recv_sem=ag_r,
                    device_id=(lax.rem(t + k, NTP), d),
                    device_id_type=MESH,
                ).start()
                return 0

            lax.fori_loop(1, NTP, push_out, 0)
        else:
            mixed_ref[...] = total[0:PER, :]

    for l in range(2):
        pltpu.make_async_copy(st.at[l], nst_hbm.at[l], out_sem.at[l]).wait()
        wait_bytes(wbuf.at[l, pl.ds(0, NDP - 1)], win_s.at[l])
        wait_bytes(wobuf.at[l, pl.ds(0, NDP - 1)], wo_s.at[l])
        wait_bytes(map_buf.at[l, pl.ds(0, NTP - 1)], map_s.at[l])
    wait_paired(lambda n: xbuf.at[0, pl.ds(0, n)], tok_s)
    wait_bytes(part_buf.at[0, pl.ds(0, NTP - 1)], part_s.at[0])
    wait_paired(lambda n: part_buf.at[1, pl.ds(0, n)], part_s.at[1])
    wait_bytes(xbuf.at[1, pl.ds(0, NTP - 1)], ag_s)


def local(
    tokens,
    lengths,
    norm_gain,
    w_gate,
    w_value,
    w_write,
    w_read,
    w_step,
    step_bias,
    decay_rate,
    skip_gain,
    conv_value_w,
    conv_write_w,
    conv_read_w,
    group_gain,
    w_out,
    state,
    hist_value,
    hist_write,
    hist_read,
):
    flip = lambda a: jnp.swapaxes(a, 1, 2)
    vmem = pl.BlockSpec(memory_space=pltpu.VMEM)
    anywhere = pl.BlockSpec(memory_space=pl.ANY)
    dma = pltpu.SemaphoreType.DMA
    mixed, new_state, nhv, nhw, nhr = pl.pallas_call(
        kernel,
        out_shape=(
            jax.ShapeDtypeStruct((PER, 128), F32),
            jax.ShapeDtypeStruct((2, SEQ, HD, ST), F32),
            jax.ShapeDtypeStruct((2, 3, SEQ, HD), BF16),
            jax.ShapeDtypeStruct((2, 3, 8, SEQ), BF16),
            jax.ShapeDtypeStruct((2, 3, 8, SEQ), BF16),
        ),
        in_specs=[vmem] * 16 + [anywhere] + [vmem] * 3,
        out_specs=(vmem, anywhere, vmem, vmem, vmem),
        scratch_shapes=[
            pltpu.VMEM((2, SEQ, HD, ST), F32),
            pltpu.VMEM((2, NTP, PAD, 128), BF16),
            pltpu.VMEM((2, NDP, NW, 128), BF16),
            pltpu.VMEM((2, NDP, HD, 128), BF16),
            pltpu.VMEM((PAD, 128), BF16),
            pltpu.VMEM((2, 2, 8, 128), BF16),
            pltpu.VMEM((2, NTP, 8, 128), BF16),
            pltpu.VMEM((2, NDP, NBLK, PAD, 128), BF16),
            pltpu.VMEM((2, NTP, PAD, 128), BF16),
            pltpu.VMEM((2, HD, ROWS), F32),
            pltpu.VMEM((2, 16, ROWS), F32),
            pltpu.VMEM((256, 256), BF16),
            pltpu.VMEM((ROWS, 2 * ST), F32),
            dma((2,)),
            dma((2,)),
            dma,
            dma,
            dma((2,)),
            dma((2,)),
            dma((2,)),
            dma((2,)),
            dma((2,)),
            dma((2,)),
            dma((2,)),
            dma((2,)),
            dma,
            dma,
        ],
        compiler_params=pltpu.CompilerParams(collective_id=0, has_side_effects=True),
        name="decode_step",
    )(
        tokens,
        lengths.reshape(1, SEQ),
        norm_gain,
        flip(w_gate),
        flip(w_value),
        flip(w_write),
        flip(w_read),
        w_step.reshape(2, 128),
        step_bias.reshape(1, 2),
        decay_rate.reshape(1, 2),
        skip_gain.reshape(1, 2),
        conv_value_w,
        conv_write_w,
        conv_read_w,
        group_gain,
        w_out,
        state.reshape(2, SEQ, HD, ST),
        flip(hist_value),
        jnp.transpose(hist_write, (0, 2, 3, 1)),
        jnp.transpose(hist_read, (0, 2, 3, 1)),
    )
    back = lambda a: jnp.transpose(a, (0, 3, 1, 2))
    return (
        mixed,
        new_state.reshape(2, SEQ, 1, HD, ST),
        flip(nhv),
        back(nhw),
        back(nhr),
    )


def solution(mesh):
    return jax.shard_map(
        local,
        mesh=mesh,
        in_specs=(
            P("tp", "dp"),
            P("dp"),
            P(None, "dp"),
            P(None, "dp", "tp"),
            P(None, "dp", "tp"),
            P(None, "dp", "tp"),
            P(None, "dp", "tp"),
            P(None, "dp", "tp"),
            P(None, "tp"),
            P(None, "tp"),
            P(None, "tp"),
            P(None, None, "tp"),
            P(None, None, "tp"),
            P(None, None, "tp"),
            P(None, "tp"),
            P(None, "tp", "dp"),
            P(None, "dp", "tp", None, None),
            P(None, "dp", None, "tp"),
            P(None, "dp", None, "tp"),
            P(None, "dp", None, "tp"),
        ),
        out_specs=(
            P("tp", "dp"),
            P(None, "dp", "tp", None, None),
            P(None, "dp", None, "tp"),
            P(None, "dp", None, "tp"),
            P(None, "dp", None, "tp"),
        ),
        check_vma=False,
    )
```

time: 471 us -> 66.3 us (0.14)
  the two profiles are of different devices: /device:TPU:2 before, /device:TPU:1 now
where the time goes in v1:
time: 66.3 us; the launch traced here: 66.1 us
  Pallas kernels  59.6 us (90%)
  local copies, waits for them, and re-layouts  5.83 us (9%)
    pallas_call x1, Pallas kernels, local(): pl.pallas_call(kernel, out_shape=(jax.ShapeDtypeStruct((PER, 128), F32),...  59.6 us
    unnamed x11, local copies, waits for them, and re-layouts  5.83 us

profile of v1, /device:TPU:1, one launch (start us, length us, event | category | flops | bytes accessed | tf_op | source)
XLA Modules:
  0.0 66.1 jit_solution(11380900671602064489)
XLA Ops:
  0.6 59.6 %decode_step.1 = (f32[6,128]{1,0:T(8,128)}, f32[2,24,64,128]{3,2,1,0:T(8,128)}, bf16[2,3,24,64]{3,2,1,0:T(8,128)(2,1)}, bf16[2,3,8,24]{3,2,1,0:T(8,128)(2,1)}, bf16[2,3,8,24]{3,2,1,0:T(8,128)(2,1)}) custom-call(bf16[6,128]{1,0:T(8,128)(2,1)} %tok_ref.1, s32[1,24]{1,0:T(1,128)} %bitcast.31, f32[2,128]{1,0:T(2,128)} %gain_ref.1, bf16[2,64,128]{2,1,0:T(8,128)(2,1)} %bitcast.23, ...), custom_call_target="tpu_custom_call" | custom-call | tf_op jit(solution)/shard_map/decode_step/pallas_call | solution.py:480
  60.3 1.3 %copy.31 = f32[6,128]{1,0:T(8,128)} copy(f32[6,128]{1,0:T(8,128)} %get-tuple-element.25) | data formatting | bytes 6144
  61.5 0.0 copy-start
  61.5 0.0 copy-start.2
  61.5 0.0 copy-start.1
  61.5 2.7 %copy.32 = f32[2,24,1,64,128]{4,3,2,1,0:T(8,128)} copy(f32[2,24,1,64,128]{4,3,2,1,0:T(8,128)} %bitcast.20) | data formatting | bytes 3145728
  64.3 0.0 copy-done
  64.3 0.6 copy.33
  64.9 0.0 copy-done.2
  64.9 0.6 copy.34
  65.5 0.0 copy-done.1
  65.5 0.6 copy.35
Async XLA Ops:
  61.5 2.7 %copy-start = (bf16[2,3,24,64]{3,2,1,0:T(8,128)(2,1)S(1)}, bf16[2,3,24,64]{3,2,1,0:T(8,128)(2,1)}, u32[]{:S(2)}) copy-start(bf16[2,3,24,64]{3,2,1,0:T(8,128)(2,1)} %get-tuple-element.12) | copy-start | bytes 55300
  61.5 3.4 %copy-start.2 = (bf16[2,3,8,24]{3,2,1,0:T(8,128)(2,1)S(1)}, bf16[2,3,8,24]{3,2,1,0:T(8,128)(2,1)}, u32[]{:S(2)}) copy-start(bf16[2,3,8,24]{3,2,1,0:T(8,128)(2,1)} %get-tuple-element.13) | copy-start | bytes 6916
  61.5 4.0 %copy-start.1 = (bf16[2,3,8,24]{3,2,1,0:T(8,128)(2,1)S(1)}, bf16[2,3,8,24]{3,2,1,0:T(8,128)(2,1)}, u32[]{:S(2)}) copy-start(bf16[2,3,8,24]{3,2,1,0:T(8,128)(2,1)} %get-tuple-element.14) | copy-start | bytes 6916

commit v2 on v1

v2 whole, which is shorter than its diff:
```python
import jax
import jax.numpy as jnp
from jax import lax
from jax.experimental import pallas as pl
from jax.experimental.pallas import tpu as pltpu
from jax.sharding import PartitionSpec as P

MESH = pl.DeviceIdType.MESH
F32 = jnp.float32
BF16 = jnp.bfloat16

NTP = 32
NZ = 8
NY = 4
NDP = 8
PER = 6
PAD = 8
NBLK = 4
ROWS = NBLK * PAD
SEQ = NBLK * PER
HD = 64
ST = 128
D = 1024
GW = 1024.0
EPS = 1e-05
NW = 160
MB = 2**20

NT = (((1,), (1,)), ((), ()))
TN = (((0,), (0,)), ((), ()))
NN = (((1,), (0,)), ((), ()))


def ring(off, n):
    return min(off, n - off)


TP_OFF = sorted(
    [(dz, dy) for dz in range(NZ) for dy in range(NY)],
    key=lambda o: -(ring(o[0], NZ) + ring(o[1], NY)),
)
DP_OFF = [4, 5, 3, 2, 6, 7, 1, 0]
LAST_OFF = sorted(
    [(dc, dy) for dc in DP_OFF for dy in range(NY)],
    key=lambda o: -(ring(o[0], NDP) / 2 + ring(o[1], NY)),
)


def dot(a, b, dims):
    return lax.dot_general(a, b, dims, preferred_element_type=F32)


def iota(shape, dim):
    return lax.broadcasted_iota(jnp.int32, shape, dim)


def silu(x):
    return x / (1.0 + jnp.exp(-x))


def column(row, rows):
    wide = jnp.broadcast_to(row, (rows, row.shape[1]))
    pick = iota(wide.shape, 1) == iota(wide.shape, 0)
    return jnp.sum(jnp.where(pick, wide, 0.0), axis=1, keepdims=True)


def split(x):
    high = x.astype(BF16).astype(F32)
    return high, x - high


def kernel(*refs):
    hbm = refs[:20]
    mixed_ref, st, nhv_ref, nhw_ref, nhr_ref = refs[20:25]
    fetched = refs[25:44]
    (
        stb,
        xbuf,
        wbuf,
        wobuf,
        tok_send,
        early_send,
        early_buf,
        wmap,
        map_send,
        map_buf,
        part_send,
        part_buf,
        pre_v,
        pre_m,
        sel,
        wr_all,
        in_sem,
        st_sem,
        tok_s,
        tok_r,
        win_s,
        win_r,
        wo_s,
        wo_r,
        early_s,
        early_r,
        wmap_s,
        wmap_r,
        map_s,
        map_r,
        part_s,
        part_r,
        ag_s,
        ag_r,
    ) = refs[44:]
    (
        tok_ref,
        len_ref,
        gain_ref,
        wg_ref,
        wv_ref,
        ww_ref,
        wr_ref,
        ws_ref,
        bias_ref,
        rate_ref,
        skip_ref,
        cv_ref,
        cw_ref,
        cr_ref,
        gg_ref,
        wo_ref,
        hv_ref,
        hw_ref,
        hr_ref,
    ) = fetched

    t = lax.axis_index("tp")
    d = lax.axis_index("dp")
    z, y = t // NY, t % NY
    mine = z == d
    others = jnp.logical_not(mine)

    small = [r for i, r in enumerate(hbm) if i != 16]
    fetches = [
        pltpu.make_async_copy(src, dst, in_sem.at[i])
        for i, (src, dst) in enumerate(zip(small, fetched))
    ]
    for copy in fetches:
        copy.start()

    def tp_at(off):
        return lax.rem(z + off[0], NZ) * NY + lax.rem(y + off[1], NY)

    def last_at(off):
        return d * NY + lax.rem(y + off[1], NY), lax.rem(d + off[0], NDP)

    barrier = pltpu.get_barrier_semaphore()

    def tell(i_tp, i_dp):
        pl.semaphore_signal(barrier, inc=1, device_id=(i_tp, i_dp), device_id_type=MESH)

    for off in TP_OFF:
        if off == (0, 0):
            pl.when(others)(lambda: tell(t, z))
        else:
            tell(tp_at(off), z)
    for off in TP_OFF[:-1]:
        tell(tp_at(off), d)
    for off in LAST_OFF:
        if off == (0, 0):
            pl.when(others)(lambda: tell(*last_at((0, 0))))
        else:
            tell(*last_at(off))
    for off in DP_OFF[:-1]:
        tell(t, lax.rem(d + off, NDP))

    st_copies = []
    for l in range(2):
        copy = pltpu.make_async_copy(hbm[16].at[l], st.at[l], st_sem.at[l])
        copy.start()
        st_copies.append(copy)

    q_r, q_c = iota((16, 16), 0), iota((16, 16), 1)
    perm = jnp.where(
        q_c == ((q_r % 8) // 4) * 8 + 2 * (q_r % 4) + q_r // 8, 1.0, 0.0
    ).astype(BF16)
    p_r, p_c = iota((SEQ, ROWS), 0), iota((SEQ, ROWS), 1)
    spread = jnp.where(p_c == (p_r // PER) * PAD + p_r % PER, 1.0, 0.0).astype(BF16)
    r8 = iota((8, 128), 0)

    for copy in fetches:
        copy.wait()

    tok_send[...] = jnp.concatenate(
        [tok_ref[...].astype(F32), jnp.zeros((PAD - PER, 128), F32)], axis=0
    ).astype(BF16)

    for l in range(2):
        maps = jnp.concatenate([ww_ref[l].astype(F32), wr_ref[l].astype(F32)], axis=0).astype(BF16)
        maps = dot(perm, maps, NN)
        high, low = split(gain_ref[l : l + 1, :])
        step_row = ws_ref[l : l + 1, :].astype(F32)
        extra = jnp.where(
            r8 == 0, step_row, jnp.where(r8 == 1, high, jnp.where(r8 == 2, low, 0.0))
        )
        packed = jnp.concatenate([maps, extra, jnp.zeros((8, 128), F32)], axis=0)
        wbuf[l, d, pl.ds(128, 32), :] = packed.astype(BF16)
        wbuf[l, d, pl.ds(0, 64), :] = wg_ref[l]
        wbuf[l, d, pl.ds(64, 64), :] = wv_ref[l]
        wobuf[l, d] = wo_ref[l]
        if l == 1:
            early_send[0, 0] = maps[0:8].astype(BF16)
            early_send[1, 0] = maps[8:16].astype(BF16)

    pl.semaphore_wait(barrier, jnp.where(mine, 31 + 7 + 62, 31 + 7 + 64))

    def send(src, dst, s_sem, r_sem, i_tp, i_dp):
        pltpu.make_async_remote_copy(
            src_ref=src,
            dst_ref=dst,
            send_sem=s_sem,
            recv_sem=r_sem,
            device_id=(i_tp, i_dp),
            device_id_type=MESH,
        ).start()

    def wait_bytes(ref, sem):
        pltpu.make_async_copy(ref, ref, sem).wait()

    def wait_paired(ref_of, sem):
        pl.when(mine)(lambda: wait_bytes(ref_of(NTP - 1), sem))
        pl.when(others)(lambda: wait_bytes(ref_of(NTP), sem))

    own_slot = d * NBLK + y

    for off in TP_OFF:
        go = lambda dest: send(tok_send, xbuf.at[0, own_slot], tok_s, tok_r, dest, z)
        if off == (0, 0):
            pl.when(others)(lambda: go(t))
        else:
            go(tp_at(off))

    @pl.when(mine)
    def _():
        xbuf[0, own_slot] = tok_send[...]

    def push_dp(ref, s_sem, r_sem):
        for off in DP_OFF[:-1]:
            send(ref, ref, s_sem, r_sem, t, lax.rem(d + off, NDP))

    for l in range(1):
        push_dp(wbuf.at[l, d], win_s.at[l], win_r.at[l])
        push_dp(wobuf.at[l, d], wo_s.at[l], wo_r.at[l])

    len_row = len_ref[...].astype(F32)
    len_pad = dot(jnp.broadcast_to(len_row, (8, SEQ)).astype(BF16), spread, NN)[0:1, :]
    len_col = column(len_row, SEQ)
    live_row = [jnp.where(len_row >= 3.0 - k, 1.0, 0.0) for k in range(3)]
    live_pad = [jnp.where(len_pad >= 3.0 - k, 1.0, 0.0) for k in range(3)]
    live_col = [jnp.where(len_col >= 3.0 - k, 1.0, 0.0) for k in range(3)]

    c_r, c_c = iota((16, 8), 0), iota((16, 8), 1)
    c_pick = c_c == 2 * (c_r % 4) + c_r // 8
    c_kind = (c_r % 8) // 4
    tap_v, tap_m, gain_col = [None, None], [None, None], [None, None]
    for l in (1, 0):
        acc_v = jnp.zeros((HD, ROWS), F32)
        acc_m = jnp.zeros((16, ROWS), F32)
        for k in range(4):
            tv = column(cv_ref[l, k : k + 1, :], HD)
            both = jnp.where(c_kind == 0, cw_ref[l, k : k + 1, :], cr_ref[l, k : k + 1, :])
            tm = jnp.sum(jnp.where(c_pick, both, 0.0), axis=1, keepdims=True)
            if k == 3:
                tap_v[l] = tv
                tap_m[l] = tm
                continue
            acc_v = acc_v + dot(hv_ref[l, k], spread, TN) * live_pad[k] * tv
            hm = jnp.concatenate(
                [hw_ref[l, k].astype(F32), hr_ref[l, k].astype(F32)], axis=0
            ).astype(BF16)
            hm = dot(perm, hm, NN).astype(BF16)
            acc_m = acc_m + dot(hm, spread, NN) * live_pad[k] * tm
        pre_v[l] = acc_v
        pre_m[l] = acc_m
        gain_col[l] = column(gg_ref[l : l + 1, :], HD)
        if l == 1:
            p_high, p_low = split(acc_m)
            t_high, t_low = split(tap_m[l])
            filler = jnp.zeros((16, 32), F32)
            wide = jnp.concatenate(
                [
                    p_high,
                    jnp.broadcast_to(t_high, (16, 32)),
                    p_low,
                    jnp.broadcast_to(t_low, (16, 32)),
                ],
                axis=1,
            )
            early_send[0, 1] = wide[0:8].astype(BF16)
            early_send[1, 1] = wide[8:16].astype(BF16)
            for off in TP_OFF[:-1]:
                dest = tp_at(off)
                send(
                    early_send.at[dest // 16],
                    early_buf.at[t],
                    early_s,
                    early_r,
                    dest,
                    d,
                )
            early_buf[t] = early_send[t // 16]

    s_r, s_c = iota((256, 256), 0), iota((256, 256), 1)
    sel[...] = jnp.where(
        s_c == ((s_r % 8) // 4) * 128 + (s_r // 8) * 4 + s_r % 4, 1.0, 0.0
    ).astype(BF16)

    for l in range(2):
        st_copies[l].wait()
        for s in range(SEQ):
            stb[l, pl.ds(s * HD, HD), :] = st[l, s].astype(BF16)

    row_of = iota((ROWS, 128), 0) % PAD
    lane32 = iota((HD, ROWS), 1)

    for l in range(2):
        if l == 0:
            wait_paired(lambda n: xbuf.at[0, pl.ds(0, n)], tok_r)
        else:
            wait_bytes(xbuf.at[1, pl.ds(0, NTP - 1)], ag_r)
        xs = []
        squares = jnp.zeros((ROWS, 128), F32)
        for c in range(NDP):
            x = xbuf[l, pl.ds(c * NBLK, NBLK)].astype(F32).reshape(ROWS, 128)
            xs.append(x)
            squares = squares + x * x
        scale = lax.rsqrt(jnp.sum(squares, axis=1, keepdims=True) / D + EPS)
        if l == 0:
            wait_bytes(wbuf.at[l, pl.ds(0, NDP - 1)], win_r.at[l])
        normed = []
        for c in range(NDP):
            gains = wbuf[l, c, pl.ds(144, 16), :].astype(F32)
            gain = gains[1:2, :] + gains[2:3, :]
            normed.append((xs[c] * scale * gain).astype(BF16))
        if l == 1:
            full = jnp.zeros((256, ROWS), F32)
            for c in range(NDP):
                full = full + dot(wmap[c], normed[c], NT)
        proj = jnp.zeros((NW, ROWS), F32)
        for c in range(NDP):
            proj = proj + dot(wbuf[l, c], normed[c], NT)
        maps_new = proj[128:144, :].astype(BF16)
        if l == 0:
            maps_act = silu(pre_m[l] + maps_new.astype(F32) * tap_m[l])
            map_send[:, :, pl.ds(0, ROWS)] = maps_act.reshape(2, 8, ROWS).astype(BF16)
            for off in TP_OFF[:-1]:
                dest = tp_at(off)
                send(map_send.at[dest // 16], map_buf.at[t], map_s, map_r, dest, d)
            map_buf[t] = map_send[t // 16]
            push_dp(wbuf.at[1, d], win_s.at[1], win_r.at[1])
            push_dp(wobuf.at[1, d], wo_s.at[1], wo_r.at[1])

        gate = proj[0:64, :].astype(BF16).astype(F32)
        value_new = proj[64:128, :].astype(BF16)
        u = silu(pre_v[l] + value_new.astype(F32) * tap_v[l])
        raw = proj[144:145, :] + bias_ref[0:1, l : l + 1]
        step = jnp.maximum(raw, 0.0) + jnp.log1p(jnp.exp(-jnp.abs(raw)))
        keep = jnp.exp(-rate_ref[0:1, l : l + 1] * step)
        su = step * u
        sgate = silu(gate)

        if l == 0:
            wait_bytes(map_buf.at[pl.ds(0, NTP - 1)], map_r)
            gathered = map_buf[...].astype(F32).reshape(NTP * 8, 128)[:, 0:ROWS].astype(BF16)
        else:
            info = early_buf[:, 1].astype(F32).reshape(NTP * 8, 128)
            hist_part = info[:, 0:32] + info[:, 64:96]
            tap = info[:, 32:64] + info[:, 96:128]
            gathered = silu(hist_part + full.astype(BF16).astype(F32) * tap).astype(BF16)
        maps_t = dot(sel[...], gathered, TN)
        read_t = maps_t[128:256, :]
        overlap = jnp.sum(maps_t[0:128, :] * read_t, axis=0, keepdims=True)

        read_b = read_t.astype(BF16)
        old = jnp.zeros((HD, ROWS), F32)
        for s in range(SEQ):
            lane = (s // PER) * PAD + s % PER
            got = dot(stb[l, pl.ds(s * HD, HD), :], read_b, NN)
            old = jnp.where(lane32 == lane, got, old)
        read_out = keep * old + su * overlap
        gated = (read_out + skip_ref[0:1, l : l + 1] * u) * sgate
        sq = jnp.sum(gated * gated, axis=0, keepdims=True)
        sq = jnp.concatenate([sq, jnp.zeros((1, 128 - ROWS), F32)], axis=1)
        sq_high, sq_low = split(sq)
        mix = (gated * gain_col[l]).astype(BF16)
        if l == 0:
            wait_bytes(wobuf.at[l, pl.ds(0, NDP - 1)], wo_r.at[l])
        for c in range(NDP):
            part = dot(mix, wobuf[l, c], TN)
            part = jnp.where(row_of == PER, sq_high, jnp.where(row_of == PER + 1, sq_low, part))
            part_send[l, pl.ds(c * NBLK, NBLK)] = part.reshape(NBLK, PAD, 128).astype(BF16)

        if l == 0:
            for off in TP_OFF[:-1]:
                dest = tp_at(off)
                send(
                    part_send.at[0, dest],
                    part_buf.at[0, t],
                    part_s.at[0],
                    part_r.at[0],
                    dest,
                    d,
                )
            part_buf[0, t] = part_send[0, t]
        else:
            for off in LAST_OFF:

                def go(i_tp, i_dp):
                    send(
                        part_send.at[1, i_dp * NBLK + i_tp % NY],
                        part_buf.at[1, t],
                        part_s.at[1],
                        part_r.at[1],
                        i_tp,
                        i_dp,
                    )

                if off == (0, 0):
                    pl.when(others)(lambda: go(*last_at((0, 0))))
                else:
                    go(*last_at(off))

            @pl.when(mine)
            def _():
                part_buf[1, t] = part_send[1, own_slot]

        if l == 0:
            wait_bytes(early_buf.at[pl.ds(0, NTP - 1)], early_r)
            rows = early_buf[:, 0].astype(F32).reshape(NTP * 8, 128).astype(BF16)
            wmap[d] = rows
            push_dp(wmap.at[d], wmap_s, wmap_r)
        wr_all[...] = dot(gathered, sel[...], TN)
        for s in range(SEQ):
            lane = (s // PER) * PAD + s % PER
            st[l, s] = (
                keep[0:1, lane : lane + 1] * st[l, s]
                + su[:, lane : lane + 1] * wr_all[lane : lane + 1, 0:ST]
            )
        for k in range(1, 3):
            nhv_ref[l, k - 1] = (hv_ref[l, k].astype(F32) * live_col[k]).astype(BF16)
            nhw_ref[l, k - 1] = (hw_ref[l, k].astype(F32) * live_row[k]).astype(BF16)
            nhr_ref[l, k - 1] = (hr_ref[l, k].astype(F32) * live_row[k]).astype(BF16)
        nhv_ref[l, 2] = dot(spread, value_new, NT).astype(BF16)
        back = dot(perm, maps_new, TN).astype(BF16)
        back = dot(back, spread, NT)
        nhw_ref[l, 2] = back[0:8].astype(BF16)
        nhr_ref[l, 2] = back[8:16].astype(BF16)

        if l == 0:
            wait_bytes(part_buf.at[0, pl.ds(0, NTP - 1)], part_r.at[0])
        else:
            wait_paired(lambda n: part_buf.at[1, pl.ds(0, n)], part_r.at[1])
        total = jnp.zeros((PAD, 128), F32)
        for grp in range(2):
            acc = part_buf[l, grp * 16].astype(F32)
            for i in range(1, 16):
                acc = acc + part_buf[l, grp * 16 + i].astype(F32)
            both = acc[PER : PER + 1, :] + acc[PER + 1 : PER + 2, :]
            wide = jnp.broadcast_to(both, (PAD, 128))
            pick = iota((PAD, 128), 1) == y * PAD + iota((PAD, 128), 0)
            mean = jnp.sum(jnp.where(pick, wide, 0.0), axis=1, keepdims=True) / GW
            total = total + acc * lax.rsqrt(mean + EPS)

        if l == 0:
            total = jnp.where(iota((PAD, 128), 0) < PER, total, 0.0)
            xbuf[1, t] = total.astype(BF16)
            for off in TP_OFF[:-1]:
                send(xbuf.at[1, t], xbuf.at[1, t], ag_s, ag_r, tp_at(off), d)
            wait_bytes(wbuf.at[1, pl.ds(0, NDP - 1)], win_r.at[1])
            wait_bytes(wobuf.at[1, pl.ds(0, NDP - 1)], wo_r.at[1])
            wait_bytes(wmap.at[pl.ds(0, NDP - 1)], wmap_r)
        else:
            mixed_ref[...] = total[0:PER, :]

    for l in range(2):
        wait_bytes(wbuf.at[l, pl.ds(0, NDP - 1)], win_s.at[l])
        wait_bytes(wobuf.at[l, pl.ds(0, NDP - 1)], wo_s.at[l])
    wait_bytes(wmap.at[pl.ds(0, NDP - 1)], wmap_s)
    wait_bytes(map_buf.at[pl.ds(0, NTP - 1)], map_s)
    wait_bytes(early_buf.at[pl.ds(0, NTP - 1)], early_s)
    wait_paired(lambda n: xbuf.at[0, pl.ds(0, n)], tok_s)
    wait_bytes(part_buf.at[0, pl.ds(0, NTP - 1)], part_s.at[0])
    wait_paired(lambda n: part_buf.at[1, pl.ds(0, n)], part_s.at[1])
    wait_bytes(xbuf.at[1, pl.ds(0, NTP - 1)], ag_s)


def write_out(*refs):
    srcs, dsts, sem = refs[:5], refs[5:10], refs[10]
    copies = [
        pltpu.make_async_copy(src, dst, sem.at[i]) for i, (src, dst) in enumerate(zip(srcs, dsts))
    ]
    for copy in copies:
        copy.start()
    for copy in copies:
        copy.wait()


def local(
    tokens,
    lengths,
    norm_gain,
    w_gate,
    w_value,
    w_write,
    w_read,
    w_step,
    step_bias,
    decay_rate,
    skip_gain,
    conv_value_w,
    conv_write_w,
    conv_read_w,
    group_gain,
    w_out,
    state,
    hist_value,
    hist_write,
    hist_read,
):
    flip = lambda a: jnp.swapaxes(a, 1, 2)
    vmem = pl.BlockSpec(memory_space=pltpu.VMEM)
    hbm = pl.BlockSpec(memory_space=pltpu.HBM)
    dma = pltpu.SemaphoreType.DMA
    operands = (
        tokens,
        lengths.reshape(1, SEQ),
        norm_gain,
        flip(w_gate),
        flip(w_value),
        flip(w_write),
        flip(w_read),
        w_step.reshape(2, 128),
        step_bias.reshape(1, 2),
        decay_rate.reshape(1, 2),
        skip_gain.reshape(1, 2),
        conv_value_w,
        conv_write_w,
        conv_read_w,
        group_gain,
        w_out,
        state.reshape(2, SEQ, HD, ST),
        flip(hist_value),
        jnp.transpose(hist_write, (0, 2, 3, 1)),
        jnp.transpose(hist_read, (0, 2, 3, 1)),
    )
    results = (
        jax.ShapeDtypeStruct((PER, 128), F32),
        jax.ShapeDtypeStruct((2, SEQ, HD, ST), F32),
        jax.ShapeDtypeStruct((2, 3, SEQ, HD), BF16),
        jax.ShapeDtypeStruct((2, 3, 8, SEQ), BF16),
        jax.ShapeDtypeStruct((2, 3, 8, SEQ), BF16),
    )
    operands = tuple(pltpu.with_memory_space_constraint(a, pltpu.HBM) for a in operands)
    made = pl.pallas_call(
        kernel,
        out_shape=results,
        in_specs=[hbm] * 20,
        out_specs=(vmem,) * 5,
        scratch_shapes=[
            pltpu.VMEM(a.shape, a.dtype) for i, a in enumerate(operands) if i != 16
        ]
        + [
            pltpu.VMEM((2, SEQ * HD, ST), BF16),
            pltpu.VMEM((2, NTP, PAD, 128), BF16),
            pltpu.VMEM((2, NDP, NW, 128), BF16),
            pltpu.VMEM((2, NDP, HD, 128), BF16),
            pltpu.VMEM((PAD, 128), BF16),
            pltpu.VMEM((2, 2, 8, 128), BF16),
            pltpu.VMEM((NTP, 2, 8, 128), BF16),
            pltpu.VMEM((NDP, 256, 128), BF16),
            pltpu.VMEM((2, 8, 128), BF16),
            pltpu.VMEM((NTP, 8, 128), BF16),
            pltpu.VMEM((2, NTP, PAD, 128), BF16),
            pltpu.VMEM((2, NTP, PAD, 128), BF16),
            pltpu.VMEM((2, HD, ROWS), F32),
            pltpu.VMEM((2, 16, ROWS), F32),
            pltpu.VMEM((256, 256), BF16),
            pltpu.VMEM((ROWS, 2 * ST), F32),
            dma((19,)),
            dma((2,)),
            dma,
            dma,
            dma((2,)),
            dma((2,)),
            dma((2,)),
            dma((2,)),
            dma,
            dma,
            dma,
            dma,
            dma,
            dma,
            dma((2,)),
            dma((2,)),
            dma,
            dma,
        ],
        compiler_params=pltpu.CompilerParams(
            collective_id=0, has_side_effects=True, vmem_limit_bytes=16 * MB
        ),
        name="decode_step",
    )(*operands)
    mixed, new_state, nhv, nhw, nhr = pl.pallas_call(
        write_out,
        out_shape=results,
        in_specs=[vmem] * 5,
        out_specs=(hbm,) * 5,
        scratch_shapes=[dma((5,))],
        compiler_params=pltpu.CompilerParams(vmem_limit_bytes=4 * MB),
        name="write_out",
    )(*made)
    back = lambda a: jnp.transpose(a, (0, 3, 1, 2))
    return (
        mixed,
        new_state.reshape(2, SEQ, 1, HD, ST),
        flip(nhv),
        back(nhw),
        back(nhr),
    )


def solution(mesh):
    return jax.shard_map(
        local,
        mesh=mesh,
        in_specs=(
            P("tp", "dp"),
            P("dp"),
            P(None, "dp"),
            P(None, "dp", "tp"),
            P(None, "dp", "tp"),
            P(None, "dp", "tp"),
            P(None, "dp", "tp"),
            P(None, "dp", "tp"),
            P(None, "tp"),
            P(None, "tp"),
            P(None, "tp"),
            P(None, None, "tp"),
            P(None, None, "tp"),
            P(None, None, "tp"),
            P(None, "tp"),
            P(None, "tp", "dp"),
            P(None, "dp", "tp", None, None),
            P(None, "dp", None, "tp"),
            P(None, "dp", None, "tp"),
            P(None, "dp", None, "tp"),
        ),
        out_specs=(
            P("tp", "dp"),
            P(None, "dp", "tp", None, None),
            P(None, "dp", None, "tp"),
            P(None, "dp", None, "tp"),
            P(None, "dp", None, "tp"),
        ),
        check_vma=False,
    )
```

time: 66.3 us -> 49.4 us (0.75)
  Pallas kernels: 59.6 us -> 48.6 us
  local copies, waits for them, and re-layouts: 5.83 us -> 0 us
    pallas_call x1 -> x2, Pallas kernels: 59.6 us -> 48.6 us  [the longest x1 47.4 us: local(): pl.pallas_call(kernel, out_shape=results, in_specs=[hbm] * 20, out_specs=...]
    unnamed x11 -> x0, local copies, waits for them, and re-layouts: 5.83 us -> none
where the time goes in v2:
time: 49.4 us; the launch traced here: 49.3 us
  Pallas kernels  48.6 us (98%)
  between operations  0.65 us (1%)
    pallas_call x1, Pallas kernels, local(): pl.pallas_call(kernel, out_shape=results, in_specs=[hbm] * 20, out_specs=...  47.4 us
    pallas_call x1, Pallas kernels, local(): pl.pallas_call(write_out, out_shape=results, in_specs=[vmem] * 5, out_spe...  1.2 us

profile of v2, /device:TPU:1, one launch (start us, length us, event | category | flops | bytes accessed | tf_op | source)
XLA Modules:
  0.0 49.3 jit_solution(14602358858682772128)
XLA Ops:
  0.6 47.4 %decode_step.1 = (f32[6,128]{1,0:T(8,128)S(1)}, f32[2,24,64,128]{3,2,1,0:T(8,128)S(1)}, bf16[2,3,24,64]{3,2,1,0:T(8,128)(2,1)S(1)}, bf16[2,3,8,24]{3,2,1,0:T(8,128)(2,1)S(1)}, bf16[2,3,8,24]{3,2,1,0:T(8,128)(2,1)S(1)}) custom-call(bf16[6,128]{1,0:T(8,128)(2,1)} %refs_0_.1, s32[1,24]{1,0:T(1,128)} %bitcast.27, f32[2,128]{1,0:T(2,128)} %refs_2_.1, ...), custom_call_target="tpu_custom_call" | custom-call | tf_op jit(solution)/shard_map/decode_step/pallas_call | solution.py:561
  48.1 1.2 %write_out.1 = (f32[6,128]{1,0:T(8,128)}, f32[2,24,64,128]{3,2,1,0:T(8,128)}, bf16[2,3,24,64]{3,2,1,0:T(8,128)(2,1)}, bf16[2,3,8,24]{3,2,1,0:T(8,128)(2,1)}, bf16[2,3,8,24]{3,2,1,0:T(8,128)(2,1)}) custom-call(f32[6,128]{1,0:T(8,128)S(1)} %get-tuple-element.15.refs_0_, f32[2,24,64,128]{3,2,1,0:T(8,128)S(1)} %get-tuple-element.16.refs_1_, ...), custom_call_target="tpu_custom_call" | custom-call | tf_op jit(solution)/shard_map/write_out/pallas_call | solution.py:610

commit v3 on v2

--- a/solution.py
+++ b/solution.py
@@ -24,6 +24,7 @@
 GW = 1024.0
 EPS = 1e-05
 NW = 160
+NX = NW + 32
 MB = 2**20
 
 NT = (((1,), (1,)), ((), ()))
@@ -40,6 +41,7 @@
     key=lambda o: -(ring(o[0], NZ) + ring(o[1], NY)),
 )
 DP_OFF = [4, 5, 3, 2, 6, 7, 1, 0]
+EVEN_OFF = [(dz, dy) for dz in (4, 2, 6, 0) for dy in (2, 1, 3, 0)]
 LAST_OFF = sorted(
     [(dc, dy) for dc in DP_OFF for dy in range(NY)],
     key=lambda o: -(ring(o[0], NDP) / 2 + ring(o[1], NY)),
@@ -84,6 +86,9 @@
         wmap,
         map_send,
         map_buf,
+        info_send,
+        info_buf,
+        pre_all,
         part_send,
         part_buf,
         pre_v,
@@ -108,6 +113,15 @@
         part_r,
         ag_s,
         ag_r,
+        wx_s,
+        wx_r,
+        info_s,
+        info_r,
+        relay_s,
+        late_sem,
+        dp_sem,
+        dpok_sem,
+        allok_sem,
     ) = refs[44:]
     (
         tok_ref,
@@ -136,6 +150,9 @@
     z, y = t // NY, t % NY
     mine = z == d
     others = jnp.logical_not(mine)
+    odd = z % 2 == 1
+    even = jnp.logical_not(odd)
+    my_slot = ((z // 2) * NY + y) * 2 + z % 2
 
     small = [r for i, r in enumerate(hbm) if i != 16]
     fetches = [
@@ -156,20 +173,18 @@
     def tell(i_tp, i_dp):
         pl.semaphore_signal(barrier, inc=1, device_id=(i_tp, i_dp), device_id_type=MESH)
 
-    for off in TP_OFF:
-        if off == (0, 0):
-            pl.when(others)(lambda: tell(t, z))
-        else:
-            tell(tp_at(off), z)
-    for off in TP_OFF[:-1]:
-        tell(tp_at(off), d)
-    for off in LAST_OFF:
-        if off == (0, 0):
-            pl.when(others)(lambda: tell(*last_at((0, 0))))
-        else:
-            tell(*last_at(off))
-    for off in DP_OFF[:-1]:
-        tell(t, lax.rem(d + off, NDP))
+    @pl.when(even)
+    def _():
+        for off in LAST_OFF:
+            if off == (0, 0):
+                pl.when(others)(lambda: tell(*last_at((0, 0))))
+            else:
+                tell(*last_at(off))
+        for off in TP_OFF[:-1]:
+            tell(tp_at(off), d)
+        for off in DP_OFF[:-1]:
+            tell(t + NY, lax.rem(d + off, NDP))
+            tell(t, lax.rem(d + off, NDP))
 
     st_copies = []
     for l in range(2):
@@ -191,6 +206,51 @@
     tok_send[...] = jnp.concatenate(
         [tok_ref[...].astype(F32), jnp.zeros((PAD - PER, 128), F32)], axis=0
     ).astype(BF16)
+
+    pl.semaphore_wait(barrier, jnp.where(odd, 16 + 16 + 7, jnp.where(mine, 15 + 15 + 7, 16 + 15 + 7)))
+
+    def send(src, dst, s_sem, r_sem, i_tp, i_dp):
+        pltpu.make_async_remote_copy(
+            src_ref=src,
+            dst_ref=dst,
+            send_sem=s_sem,
+            recv_sem=r_sem,
+            device_id=(i_tp, i_dp),
+            device_id_type=MESH,
+        ).start()
+
+    def wait_bytes(ref, sem):
+        pltpu.make_async_copy(ref, ref, sem).wait()
+
+    def wait_paired(ref_of, sem, paired):
+        pl.when(paired)(lambda: wait_bytes(ref_of(NTP - 1), sem))
+        pl.when(jnp.logical_not(paired))(lambda: wait_bytes(ref_of(NTP), sem))
+
+    own_slot = d * NBLK + y
+    to_self = jnp.logical_and(mine, even)
+
+    for off in EVEN_OFF:
+        go = lambda dest: send(tok_send, xbuf.at[0, own_slot], tok_s, tok_r, dest, z)
+        dest = lax.rem(z + z % 2 + off[0], NZ) * NY + lax.rem(y + off[1], NY)
+        if off == (0, 0):
+            pl.when(jnp.logical_not(to_self))(lambda: go(dest))
+        else:
+            go(dest)
+
+    @pl.when(to_self)
+    def _():
+        xbuf[0, own_slot] = tok_send[...]
+
+    @pl.when(odd)
+    def _():
+        def tell_on(sem, i_tp, i_dp):
+            pl.semaphore_signal(sem, inc=1, device_id=(i_tp, i_dp), device_id_type=MESH)
+
+        for off in DP_OFF:
+            tell_on(dp_sem, t - NY, lax.rem(d + off, NDP))
+        for off in EVEN_OFF:
+            dest = lax.rem(z + 1 + off[0], NZ) * NY + lax.rem(y + off[1], NY)
+            tell_on(late_sem, dest, d)
 
     for l in range(2):
         maps = jnp.concatenate([ww_ref[l].astype(F32), wr_ref[l].astype(F32)], axis=0).astype(BF16)
@@ -209,45 +269,28 @@
             early_send[0, 0] = maps[0:8].astype(BF16)
             early_send[1, 0] = maps[8:16].astype(BF16)
 
-    pl.semaphore_wait(barrier, jnp.where(mine, 31 + 7 + 62, 31 + 7 + 64))
-
-    def send(src, dst, s_sem, r_sem, i_tp, i_dp):
-        pltpu.make_async_remote_copy(
-            src_ref=src,
-            dst_ref=dst,
-            send_sem=s_sem,
-            recv_sem=r_sem,
-            device_id=(i_tp, i_dp),
-            device_id_type=MESH,
-        ).start()
-
-    def wait_bytes(ref, sem):
-        pltpu.make_async_copy(ref, ref, sem).wait()
-
-    def wait_paired(ref_of, sem):
-        pl.when(mine)(lambda: wait_bytes(ref_of(NTP - 1), sem))
-        pl.when(others)(lambda: wait_bytes(ref_of(NTP), sem))
-
-    own_slot = d * NBLK + y
-
-    for off in TP_OFF:
-        go = lambda dest: send(tok_send, xbuf.at[0, own_slot], tok_s, tok_r, dest, z)
-        if off == (0, 0):
-            pl.when(others)(lambda: go(t))
-        else:
-            go(tp_at(off))
-
-    @pl.when(mine)
+    def push_dp(src, dst, s_sem, r_sem):
+        for off in DP_OFF[:-1]:
+            send(src, dst, s_sem, r_sem, t, lax.rem(d + off, NDP))
+
+    def push_weights(l):
+        part = wbuf.at[l, d, pl.ds(0, NW)]
+        push_dp(part, part, win_s.at[l], win_r.at[l])
+        push_dp(wobuf.at[l, d], wobuf.at[l, d], wo_s.at[l], wo_r.at[l])
+
+    pl.when(even)(lambda: push_weights(0))
+
+    @pl.when(odd)
     def _():
-        xbuf[0, own_slot] = tok_send[...]
-
-    def push_dp(ref, s_sem, r_sem):
-        for off in DP_OFF[:-1]:
-            send(ref, ref, s_sem, r_sem, t, lax.rem(d + off, NDP))
-
-    for l in range(1):
-        push_dp(wbuf.at[l, d], win_s.at[l], win_r.at[l])
-        push_dp(wobuf.at[l, d], wo_s.at[l], wo_r.at[l])
+        for off in DP_OFF:
+            send(
+                wbuf.at[0, d, pl.ds(128, 32)],
+                wbuf.at[0, d, pl.ds(NW, 32)],
+                wx_s,
+                wx_r,
+                t - NY,
+                lax.rem(d + off, NDP),
+            )
 
     len_row = len_ref[...].astype(F32)
     len_pad = dot(jnp.broadcast_to(len_row, (8, SEQ)).astype(BF16), spread, NN)[0:1, :]
@@ -260,7 +303,7 @@
     c_pick = c_c == 2 * (c_r % 4) + c_r // 8
     c_kind = (c_r % 8) // 4
     tap_v, tap_m, gain_col = [None, None], [None, None], [None, None]
-    for l in (1, 0):
+    for l in range(2):
         acc_v = jnp.zeros((HD, ROWS), F32)
         acc_m = jnp.zeros((16, ROWS), F32)
         for k in range(4):
@@ -280,36 +323,32 @@
         pre_v[l] = acc_v
         pre_m[l] = acc_m
         gain_col[l] = column(gg_ref[l : l + 1, :], HD)
-        if l == 1:
-            p_high, p_low = split(acc_m)
-            t_high, t_low = split(tap_m[l])
-            filler = jnp.zeros((16, 32), F32)
-            wide = jnp.concatenate(
-                [
-                    p_high,
-                    jnp.broadcast_to(t_high, (16, 32)),
-                    p_low,
-                    jnp.broadcast_to(t_low, (16, 32)),
-                ],
-                axis=1,
+        p_high, p_low = split(acc_m)
+        t_high, t_low = split(tap_m[l])
+        wide = jnp.concatenate(
+            [
+                p_high,
+                jnp.broadcast_to(t_high, (16, 32)),
+                p_low,
+                jnp.broadcast_to(t_low, (16, 32)),
+            ],
+            axis=1,
+        ).astype(BF16)
+        if l == 0:
+            info_send[...] = wide
+            pl.when(odd)(
+                lambda: send(info_send, info_buf, info_s, info_r, t - NY, d)
             )
+        else:
+            wide = wide.astype(F32)
             early_send[0, 1] = wide[0:8].astype(BF16)
             early_send[1, 1] = wide[8:16].astype(BF16)
-            for off in TP_OFF[:-1]:
-                dest = tp_at(off)
-                send(
-                    early_send.at[dest // 16],
-                    early_buf.at[t],
-                    early_s,
-                    early_r,
-                    dest,
-                    d,
-                )
-            early_buf[t] = early_send[t // 16]
 
     s_r, s_c = iota((256, 256), 0), iota((256, 256), 1)
+    s_p = s_r // 8
+    s_t = ((s_p // 8) * 2 + s_p % 2) * NY + (s_p // 2) % NY
     sel[...] = jnp.where(
-        s_c == ((s_r % 8) // 4) * 128 + (s_r // 8) * 4 + s_r % 4, 1.0, 0.0
+        s_c == ((s_r % 8) // 4) * 128 + s_t * 4 + s_r % 4, 1.0, 0.0
     ).astype(BF16)
 
     for l in range(2):
@@ -317,12 +356,33 @@
         for s in range(SEQ):
             stb[l, pl.ds(s * HD, HD), :] = st[l, s].astype(BF16)
 
+    @pl.when(even)
+    def _():
+        pl.semaphore_wait(dp_sem, NDP)
+        pl.semaphore_signal(dpok_sem, inc=1, device_id=(t + NY, d), device_id_type=MESH)
+        pl.semaphore_wait(late_sem, 16)
+        pl.semaphore_signal(allok_sem, inc=1, device_id=(t + NY, d), device_id_type=MESH)
+
+    @pl.when(odd)
+    def _():
+        pl.semaphore_wait(dpok_sem, 1)
+        push_weights(0)
+        pl.semaphore_wait(allok_sem, 1)
+
+    for off in TP_OFF[:-1]:
+        dest = tp_at(off)
+        send(early_send.at[dest // 16], early_buf.at[my_slot], early_s, early_r, dest, d)
+    early_buf[my_slot] = early_send[t // 16]
+
     row_of = iota((ROWS, 128), 0) % PAD
     lane32 = iota((HD, ROWS), 1)
 
     for l in range(2):
         if l == 0:
-            wait_paired(lambda n: xbuf.at[0, pl.ds(0, n)], tok_r)
+            wait_paired(lambda n: xbuf.at[0, pl.ds(0, n)], tok_r, to_self)
+            pl.when(even)(
+                lambda: send(xbuf.at[0], xbuf.at[0], relay_s, tok_r, t + NY, d)
+            )
         else:
             wait_bytes(xbuf.at[1, pl.ds(0, NTP - 1)], ag_r)
         xs = []
@@ -333,7 +393,8 @@
             squares = squares + x * x
         scale = lax.rsqrt(jnp.sum(squares, axis=1, keepdims=True) / D + EPS)
         if l == 0:
-            wait_bytes(wbuf.at[l, pl.ds(0, NDP - 1)], win_r.at[l])
+            wait_bytes(wbuf.at[l, pl.ds(0, NDP - 1), pl.ds(0, NW)], win_r.at[l])
+            pl.when(even)(lambda: wait_bytes(wbuf.at[0, :, pl.ds(NW, 32)], wx_r))
         normed = []
         for c in range(NDP):
             gains = wbuf[l, c, pl.ds(144, 16), :].astype(F32)
@@ -343,19 +404,37 @@
             full = jnp.zeros((256, ROWS), F32)
             for c in range(NDP):
                 full = full + dot(wmap[c], normed[c], NT)
-        proj = jnp.zeros((NW, ROWS), F32)
+        rows = NX if l == 0 else NW
+        proj = jnp.zeros((rows, ROWS), F32)
         for c in range(NDP):
-            proj = proj + dot(wbuf[l, c], normed[c], NT)
+            proj = proj + dot(wbuf[l, c, pl.ds(0, rows)], normed[c], NT)
         maps_new = proj[128:144, :].astype(BF16)
         if l == 0:
-            maps_act = silu(pre_m[l] + maps_new.astype(F32) * tap_m[l])
-            map_send[:, :, pl.ds(0, ROWS)] = maps_act.reshape(2, 8, ROWS).astype(BF16)
-            for off in TP_OFF[:-1]:
-                dest = tp_at(off)
-                send(map_send.at[dest // 16], map_buf.at[t], map_s, map_r, dest, d)
-            map_buf[t] = map_send[t // 16]
-            push_dp(wbuf.at[1, d], win_s.at[1], win_r.at[1])
-            push_dp(wobuf.at[1, d], wo_s.at[1], wo_r.at[1])
+
+            @pl.when(even)
+            def _():
+                own = silu(pre_m[0] + maps_new.astype(F32) * tap_m[0])
+                wait_bytes(info_buf, info_r)
+                info = info_buf[...].astype(F32)
+                theirs = proj[NW : NW + 16, :].astype(BF16).astype(F32)
+                theirs = silu(
+                    info[:, 0:32] + info[:, 64:96] + theirs * (info[:, 32:64] + info[:, 96:128])
+                )
+                map_send[:, 0, :, pl.ds(0, ROWS)] = own.reshape(2, 8, ROWS).astype(BF16)
+                map_send[:, 1, :, pl.ds(0, ROWS)] = theirs.reshape(2, 8, ROWS).astype(BF16)
+                for off in TP_OFF[:-1]:
+                    dest = tp_at(off)
+                    send(
+                        map_send.at[dest // 16],
+                        map_buf.at[pl.ds(my_slot, 2)],
+                        map_s,
+                        map_r,
+                        dest,
+                        d,
+                    )
+                map_buf[pl.ds(my_slot, 2)] = map_send[t // 16]
+
+            push_weights(1)
 
         gate = proj[0:64, :].astype(BF16).astype(F32)
         value_new = proj[64:128, :].astype(BF16)
@@ -367,14 +446,12 @@
         sgate = silu(gate)
 
         if l == 0:
-            wait_bytes(map_buf.at[pl.ds(0, NTP - 1)], map_r)
+            pl.when(even)(lambda: wait_bytes(map_buf.at[pl.ds(0, NTP - 2)], map_r))
+            pl.when(odd)(lambda: wait_bytes(map_buf, map_r))
             gathered = map_buf[...].astype(F32).reshape(NTP * 8, 128)[:, 0:ROWS].astype(BF16)
+            maps_t = dot(sel[...], gathered, TN)
         else:
-            info = early_buf[:, 1].astype(F32).reshape(NTP * 8, 128)
-            hist_part = info[:, 0:32] + info[:, 64:96]
-            tap = info[:, 32:64] + info[:, 96:128]
-            gathered = silu(hist_part + full.astype(BF16).astype(F32) * tap).astype(BF16)
-        maps_t = dot(sel[...], gathered, TN)
+            maps_t = silu(pre_all[:, 0:ROWS] + full.astype(BF16).astype(F32) * pre_all[:, ROWS:])
         read_t = maps_t[128:256, :]
         overlap = jnp.sum(maps_t[0:128, :] * read_t, axis=0, keepdims=True)
 
@@ -434,14 +511,17 @@
         if l == 0:
             wait_bytes(early_buf.at[pl.ds(0, NTP - 1)], early_r)
             rows = early_buf[:, 0].astype(F32).reshape(NTP * 8, 128).astype(BF16)
-            wmap[d] = rows
-            push_dp(wmap.at[d], wmap_s, wmap_r)
-        wr_all[...] = dot(gathered, sel[...], TN)
+            wmap[d] = dot(sel[...], rows, TN).astype(BF16)
+            push_dp(wmap.at[d], wmap.at[d], wmap_s, wmap_r)
+            info = early_buf[:, 1].astype(F32).reshape(NTP * 8, 128).astype(BF16)
+            info = dot(sel[...], info, TN)
+            pre_all[...] = info[:, 0:64] + info[:, 64:128]
+        wr_all[...] = jnp.transpose(maps_t[0:ST, :])
         for s in range(SEQ):
             lane = (s // PER) * PAD + s % PER
             st[l, s] = (
                 keep[0:1, lane : lane + 1] * st[l, s]
-                + su[:, lane : lane + 1] * wr_all[lane : lane + 1, 0:ST]
+                + su[:, lane : lane + 1] * wr_all[lane : lane + 1, :]
             )
         for k in range(1, 3):
             nhv_ref[l, k - 1] = (hv_ref[l, k].astype(F32) * live_col[k]).astype(BF16)
@@ -456,7 +536,7 @@
         if l == 0:
             wait_bytes(part_buf.at[0, pl.ds(0, NTP - 1)], part_r.at[0])
         else:
-            wait_paired(lambda n: part_buf.at[1, pl.ds(0, n)], part_r.at[1])
+            wait_paired(lambda n: part_buf.at[1, pl.ds(0, n)], part_r.at[1], mine)
         total = jnp.zeros((PAD, 128), F32)
         for grp in range(2):
             acc = part_buf[l, grp * 16].astype(F32)
@@ -473,21 +553,31 @@
             xbuf[1, t] = total.astype(BF16)
             for off in TP_OFF[:-1]:
                 send(xbuf.at[1, t], xbuf.at[1, t], ag_s, ag_r, tp_at(off), d)
-            wait_bytes(wbuf.at[1, pl.ds(0, NDP - 1)], win_r.at[1])
+            wait_bytes(wbuf.at[1, pl.ds(0, NDP - 1), pl.ds(0, NW)], win_r.at[1])
             wait_bytes(wobuf.at[1, pl.ds(0, NDP - 1)], wo_r.at[1])
             wait_bytes(wmap.at[pl.ds(0, NDP - 1)], wmap_r)
         else:
             mixed_ref[...] = total[0:PER, :]
 
     for l in range(2):
-        wait_bytes(wbuf.at[l, pl.ds(0, NDP - 1)], win_s.at[l])
+        wait_bytes(wbuf.at[l, pl.ds(0, NDP - 1), pl.ds(0, NW)], win_s.at[l])
         wait_bytes(wobuf.at[l, pl.ds(0, NDP - 1)], wo_s.at[l])
     wait_bytes(wmap.at[pl.ds(0, NDP - 1)], wmap_s)
-    wait_bytes(map_buf.at[pl.ds(0, NTP - 1)], map_s)
+    @pl.when(even)
+    def _():
+        wait_bytes(early_buf.at[pl.ds(0, NTP - 1)], map_s)
+        wait_bytes(xbuf.at[0], relay_s)
+
+    @pl.when(odd)
+    def _():
+        wait_bytes(wbuf.at[0, :, pl.ds(NW, 32)], wx_s)
+        wait_bytes(info_buf, info_s)
+
+    pl.when(to_self)(lambda: wait_bytes(xbuf.at[0, pl.ds(0, 15)], tok_s))
+    pl.when(jnp.logical_not(to_self))(lambda: wait_bytes(xbuf.at[0, pl.ds(0, 16)], tok_s))
     wait_bytes(early_buf.at[pl.ds(0, NTP - 1)], early_s)
-    wait_paired(lambda n: xbuf.at[0, pl.ds(0, n)], tok_s)
     wait_bytes(part_buf.at[0, pl.ds(0, NTP - 1)], part_s.at[0])
-    wait_paired(lambda n: part_buf.at[1, pl.ds(0, n)], part_s.at[1])
+    wait_paired(lambda n: part_buf.at[1, pl.ds(0, n)], part_s.at[1], mine)
     wait_bytes(xbuf.at[1, pl.ds(0, NTP - 1)], ag_s)
 
 
@@ -528,6 +618,7 @@
     vmem = pl.BlockSpec(memory_space=pltpu.VMEM)
     hbm = pl.BlockSpec(memory_space=pltpu.HBM)
     dma = pltpu.SemaphoreType.DMA
+    regular = pltpu.SemaphoreType.REGULAR
     operands = (
         tokens,
         lengths.reshape(1, SEQ),
@@ -569,20 +660,23 @@
         + [
             pltpu.VMEM((2, SEQ * HD, ST), BF16),
             pltpu.VMEM((2, NTP, PAD, 128), BF16),
-            pltpu.VMEM((2, NDP, NW, 128), BF16),
+            pltpu.VMEM((2, NDP, NX, 128), BF16),
             pltpu.VMEM((2, NDP, HD, 128), BF16),
             pltpu.VMEM((PAD, 128), BF16),
             pltpu.VMEM((2, 2, 8, 128), BF16),
             pltpu.VMEM((NTP, 2, 8, 128), BF16),
             pltpu.VMEM((NDP, 256, 128), BF16),
-            pltpu.VMEM((2, 8, 128), BF16),
+            pltpu.VMEM((2, 2, 8, 128), BF16),
             pltpu.VMEM((NTP, 8, 128), BF16),
+            pltpu.VMEM((16, 128), BF16),
+            pltpu.VMEM((16, 128), BF16),
+            pltpu.VMEM((256, 2 * ROWS), F32),
             pltpu.VMEM((2, NTP, PAD, 128), BF16),
             pltpu.VMEM((2, NTP, PAD, 128), BF16),
             pltpu.VMEM((2, HD, ROWS), F32),
             pltpu.VMEM((2, 16, ROWS), F32),
             pltpu.VMEM((256, 256), BF16),
-            pltpu.VMEM((ROWS, 2 * ST), F32),
+            pltpu.VMEM((ROWS, ST), F32),
             dma((19,)),
             dma((2,)),
             dma,
@@ -601,6 +695,15 @@
             dma((2,)),
             dma,
             dma,
+            dma,
+            dma,
+            dma,
+            dma,
+            dma,
+            regular,
+            regular,
+            regular,
+            regular,
         ],
         compiler_params=pltpu.CompilerParams(
             collective_id=0, has_side_effects=True, vmem_limit_bytes=16 * MB

time: 49.4 us -> 49.4 us (level)
  no operation moved by 1% of the time
where the time goes in v3:
time: 49.4 us; the launch traced here: 49.3 us
  Pallas kernels  48.6 us (98%)
  between operations  0.65 us (1%)
    pallas_call x1, Pallas kernels, local(): pl.pallas_call(kernel, out_shape=results, in_specs=[hbm] * 20, out_specs=...  47.4 us
    pallas_call x1, Pallas kernels, local(): pl.pallas_call(write_out, out_shape=results, in_specs=[vmem] * 5, out_spe...  1.2 us

profile of v3, /device:TPU:1, one launch (start us, length us, event | category | flops | bytes accessed | tf_op | source)
XLA Modules:
  0.0 49.3 jit_solution(16514924659209519057)
XLA Ops:
  0.6 47.4 %decode_step.1 = (f32[6,128]{1,0:T(8,128)S(1)}, f32[2,24,64,128]{3,2,1,0:T(8,128)S(1)}, bf16[2,3,24,64]{3,2,1,0:T(8,128)(2,1)S(1)}, bf16[2,3,8,24]{3,2,1,0:T(8,128)(2,1)S(1)}, bf16[2,3,8,24]{3,2,1,0:T(8,128)(2,1)S(1)}) custom-call(bf16[6,128]{1,0:T(8,128)(2,1)} %refs_0_.1, s32[1,24]{1,0:T(1,128)} %bitcast.27, f32[2,128]{1,0:T(2,128)} %refs_2_.1, ...), custom_call_target="tpu_custom_call" | custom-call | tf_op jit(solution)/shard_map/decode_step/pallas_call | solution.py:652
  48.1 1.2 %write_out.1 = (f32[6,128]{1,0:T(8,128)}, f32[2,24,64,128]{3,2,1,0:T(8,128)}, bf16[2,3,24,64]{3,2,1,0:T(8,128)(2,1)}, bf16[2,3,8,24]{3,2,1,0:T(8,128)(2,1)}, bf16[2,3,8,24]{3,2,1,0:T(8,128)(2,1)}) custom-call(f32[6,128]{1,0:T(8,128)S(1)} %get-tuple-element.15.refs_0_, f32[2,24,64,128]{3,2,1,0:T(8,128)S(1)} %get-tuple-element.16.refs_1_, ...), custom_call_target="tpu_custom_call" | custom-call | tf_op jit(solution)/shard_map/write_out/pallas_call | solution.py:713
